TPU v7x, 32 devices: a whole 2x2x4 slice. The times are simulated.
32 devices in a mesh: sp: 4 (over z), fs: 4 (over y, x), tp: 2 (over core).
Axes of the slice: x: 2, y: 2, z: 4, core: 2. Of those that a mesh axis runs over, the one named last changes fastest.
Arguments:
- tokens: bfloat16 [4, 1024, 2048], P('fs', ('sp', 'tp')), may hold values from -6 to 6
- norm_gain: float32 [2048], replicated, may hold values from 0.1 to 1.9
- w_query: bfloat16 [2048, 1024], P('fs', 'tp'), may hold values from -0.125 to 0.125
- w_key: bfloat16 [2048, 1024], P('fs', 'tp'), may hold values from -0.125 to 0.125
- w_value: bfloat16 [2048, 1024], P('fs', 'tp'), may hold values from -0.125 to 0.125
- w_conv_value: bfloat16 [2048, 1024], P('fs', 'tp'), may hold values from -2 to 2
- w_conv_gate: bfloat16 [2048, 1024], P('fs', 'tp'), may hold values from -0.125 to 0.125
- key_offset: bfloat16 [1024, 16], P('sp', 'tp'), may hold values from -16 to 2
- conv_kernel: float32 [31, 1024], P(None, 'tp'), may hold values from -3 to 3
- conv_gain: float32 [1024], P('tp'), may hold values from 0.1 to 1.9
- w_attn_out: bfloat16 [1024, 2048], P('tp', 'fs'), may hold values from -1 to 1
- w_conv_out: bfloat16 [1024, 2048], P('tp', 'fs'), may hold values from -0.1875 to 0.1875
Outputs:
- mixed: bfloat16 [4, 1024, 2048], P('fs', ('sp', 'tp'))
All inputs are finite; a program needn't handle non-finite values.
Results may differ from a plain program's by a relative error of at most 0.0085.
Values may be sent and summed in bfloat16 or wider, within the bound.
A program may use at most 128 MiB of HBM per device.

v0:
```python
import jax
import jax.numpy as jnp
from jax import lax
from jax.sharding import PartitionSpec as P

HD = 64
CC = 1024


def shifted(block, axis, distance):
    devices = range(lax.axis_size(axis))
    route = [(i - distance, i) for i in devices if i - distance in devices]
    return lax.ppermute(block, axis, route)


def piece_terms(queries, key_rows, value_rows, offsets, carry_log, allowed):
    head_size = queries.shape[2]
    logits = jnp.einsum(
        "qhd,khd->hqk", queries, key_rows, preferred_element_type=jnp.float32
    ) * head_size ** (-0.5)
    logits = logits + jnp.transpose(offsets.astype(jnp.float32))[:, None, :]
    log_keep = jax.nn.log_sigmoid(-logits)
    if allowed is not None:
        log_keep = jnp.where(allowed[None], log_keep, 0.0)
    between = lax.cumsum(log_keep, axis=2, reverse=True) - log_keep
    weights = jnp.exp(jax.nn.log_sigmoid(logits) + between + carry_log[:, :, None])
    if allowed is not None:
        weights = jnp.where(allowed[None], weights, 0.0)
    result = jnp.einsum(
        "hqk,khd->qhd", weights.astype(jnp.bfloat16), value_rows, preferred_element_type=jnp.float32
    )
    return (result, carry_log + jnp.sum(log_keep, axis=2))


def shards(
    tokens,
    norm_gain,
    w_query,
    w_key,
    w_value,
    w_conv_value,
    w_conv_gate,
    key_offset,
    conv_kernel,
    conv_gain,
    w_attn_out,
    w_conv_out,
):
    gathered = (
        lax.all_gather(w_query, "fs", axis=0, tiled=True),
        lax.all_gather(w_key, "fs", axis=0, tiled=True),
        lax.all_gather(w_value, "fs", axis=0, tiled=True),
        lax.all_gather(w_conv_value, "fs", axis=0, tiled=True),
        lax.all_gather(w_conv_gate, "fs", axis=0, tiled=True),
    )
    floats = lax.all_gather(tokens[0], "tp", axis=0, tiled=True).astype(jnp.float32)
    normed = (
        floats * lax.rsqrt(jnp.mean(floats * floats, axis=1, keepdims=True) + 1e-06) * norm_gain
    ).astype(jnp.bfloat16)
    projected = jnp.concatenate(
        [
            jnp.dot(normed, weight, preferred_element_type=jnp.float32).astype(jnp.bfloat16)
            for weight in gathered
        ],
        axis=1,
    )
    head_cols = w_query.shape[1]
    channels = w_conv_value.shape[1]
    block_len = projected.shape[0]
    local_heads = head_cols // HD
    queries = projected[:, :head_cols].reshape(block_len, local_heads, HD)
    key_flat = projected[:, head_cols : 2 * head_cols]
    value_flat = projected[:, 2 * head_cols : 3 * head_cols]
    conv_value = projected[:, 3 * head_cols : 3 * head_cols + channels]
    conv_gate = projected[:, 3 * head_cols + channels :]
    position = lax.axis_index("sp")
    positions = jnp.arange(block_len, dtype=jnp.int32)
    causal = positions[None, :] < positions[:, None]
    start_log = jnp.zeros((local_heads, block_len), jnp.float32)
    totals, carry_log = piece_terms(
        queries,
        key_flat.reshape(block_len, local_heads, HD),
        value_flat.reshape(block_len, local_heads, HD),
        key_offset,
        start_log,
        causal,
    )

    def visit(hop_count, carried):
        running, running_log, moving = carried
        moving = shifted((moving[0], moving[1], moving[2]), "sp", 1)
        result, next_log = piece_terms(
            queries,
            moving[0].reshape(block_len, local_heads, HD),
            moving[1].reshape(block_len, local_heads, HD),
            moving[2],
            running_log,
            None,
        )
        active = position >= hop_count
        running = jnp.where(active, running + result, running)
        running_log = jnp.where(active, next_log, running_log)
        return (running, running_log, moving)

    totals, carry_log, leftover = lax.fori_loop(
        1, lax.axis_size("sp"), visit, (totals, carry_log, (key_flat, value_flat, key_offset))
    )
    attn_heads = totals.reshape(block_len, head_cols).astype(jnp.bfloat16)
    gated_input = (
        conv_value.astype(jnp.float32) * jax.nn.sigmoid(conv_gate.astype(jnp.float32))
    ).astype(jnp.bfloat16)
    kernel_len = conv_kernel.shape[0]
    edge_rows = shifted(gated_input[block_len - (kernel_len - 1) :], "sp", 1)
    extended = jnp.concatenate([edge_rows, gated_input], axis=0).astype(jnp.float32)
    conv_sum = jnp.zeros((block_len, channels), jnp.float32)
    for tap_index in range(kernel_len):
        conv_sum = conv_sum + conv_kernel[tap_index] * extended[tap_index : tap_index + block_len]
    channel_total = lax.psum(jnp.sum(conv_sum, axis=1), "tp")
    centred = conv_sum - (channel_total / CC)[:, None]
    spread = lax.psum(jnp.sum(centred * centred, axis=1), "tp") / CC
    conv_hidden = jax.nn.silu(centred * lax.rsqrt(spread + 1e-06)[:, None] * conv_gain).astype(
        jnp.bfloat16
    )
    attn_weight, conv_weight = (
        lax.all_gather(w_attn_out, "fs", axis=1, tiled=True),
        lax.all_gather(w_conv_out, "fs", axis=1, tiled=True),
    )
    partial_value = jnp.dot(attn_heads, attn_weight, preferred_element_type=jnp.float32)
    partial_value = partial_value + jnp.dot(
        conv_hidden, conv_weight, preferred_element_type=jnp.float32
    )
    mixed = lax.psum_scatter(
        lax.optimization_barrier(partial_value.astype(jnp.bfloat16))
        .astype(jnp.float32)
        .astype(jnp.bfloat16),
        "tp",
        scatter_dimension=0,
        tiled=True,
    )
    return mixed[None]


def solution(mesh):
    placed = (
        P("fs", ("sp", "tp"), None),
        P(),
        P("fs", "tp"),
        P("fs", "tp"),
        P("fs", "tp"),
        P("fs", "tp"),
        P("fs", "tp"),
        P("sp", "tp"),
        P(None, "tp"),
        P("tp"),
        P("tp", "fs"),
        P("tp", "fs"),
    )
    return jax.shard_map(
        shards, mesh=mesh, in_specs=placed, out_specs=P("fs", ("sp", "tp"), None), check_vma=False
    )
```

profile of v0, /device:TPU:0, one launch (start us, length us, event | category | flops | bytes accessed | tf_op | source)
XLA Modules:
  0.0 299.0 jit_solution(5581829383687310881)
XLA Ops:
  12.2 8.5 %all-gather.24.cloned.1.call-done = bf16[1,256,2048]{2,1,0:T(8,128)(2,1)} async-done(((bf16[1,128,2048]{2,1,0:T(8,128)(2,1)}), bf16[1,256,2048]{2,1,0:T(8,128)(2,1)}) %all-gather.24.cloned.1.call-update) | async-done | bytes 1048592 | tf_op jit(solution)/shard_map/all_gather | solution.py:56
  22.2 36.7 %all-gather.12.cloned.1.call-done = bf16[2048,512]{1,0:T(8,128)(2,1)} async-done(((bf16[512,512]{1,0:T(8,128)(2,1)}), bf16[2048,512]{1,0:T(8,128)(2,1)}) %all-gather.12.cloned.1.call-update) | async-done | bytes 2097168 | tf_op jit(solution)/shard_map/all_gather | solution.py:50
  61.7 34.2 %all-gather.14.cloned.1.call-done = bf16[2048,512]{1,0:T(8,128)(2,1)} async-done(((bf16[512,512]{1,0:T(8,128)(2,1)}), bf16[2048,512]{1,0:T(8,128)(2,1)}) %all-gather.14.cloned.1.call-update) | async-done | bytes 2097168 | tf_op jit(solution)/shard_map/all_gather | solution.py:51
  100.9 5.1 %fusion.22 = f32[8,256,2,128]{1,0,3,2:T(8,128)S(1)} fusion(f32[8,256,2,128]{1,3,2,0:T(8,128)S(1)} %bitcast.115), kind=kOutput, calls=%fused_computation.40 | output fusion | flops 66584576 | bytes 4194304 | tf_op jit(solution)/shard_map/reduce-window
  109.8 23.1 %all-gather.10.cloned.1.call-done = bf16[2048,512]{1,0:T(8,128)(2,1)} async-done(((bf16[512,512]{1,0:T(8,128)(2,1)}), bf16[2048,512]{1,0:T(8,128)(2,1)}) %all-gather.10.cloned.1.call-update) | async-done | bytes 2097168 | tf_op jit(solution)/shard_map/all_gather | solution.py:52
  135.7 69.0 %while.21 = (s32[]{:T(128)}, f32[256,8,64]{0,2,1:T(8,128)S(1)}, f32[8,256]{1,0:T(8,128)S(1)}, bf16[256,512]{0,1:T(8,128)(2,1)S(1)}, bf16[256,512]{0,1:T(8,128)(2...) while((s32[]{:T(128)}, f32[256,8,64]{0,2,1:T(8,128)S(1)}, ...), condition=%wide.region_8.9_spmd, body=%wide.region_4.0_spmd.sunk | while | flops 224604160 | bytes 30535900 | solution.py:105
  135.9 3.4 %collective-permute-start.2 = (bf16[256,512]{0,1:T(8,128)(2,1)S(1)}, bf16[256,512]{0,1:T(8,128)(2,1)S(1)}, u32[]{:S(2)}, u32[]{:S(2)}) collective-permute-start(bf16[256,512]{0,1:T(8,128)(2,1)S(1)} %get-tuple-element.287), channel_id=1, source_target_pairs={{0,8},{8,16},{16,24},{1,9},{9,17},{17,25},{2,10},{10,18},{18,26},{... | collective-permute-start | bytes 786440 | tf_op jit(solution)/shard_map/while/body/eval_jaxpr/ppermute | solution.py:13
  139.3 3.4 %collective-permute-start.1 = (bf16[256,8]{0,1:T(8,128)(2,1)S(1)}, bf16[256,8]{0,1:T(8,128)(2,1)S(1)}, u32[]{:S(2)}, u32[]{:S(2)}) collective-permute-start(bf16[256,8]{0,1:T(8,128)(2,1)S(1)} %get-tuple-element.289), channel_id=1, source_target_pairs={{0,8},{8,16},{16,24},{1,9},{9,17},{17,25},{2,10},{10,18},{18,26},{... | collective-permute-start | bytes 12296 | tf_op jit(solution)/shard_map/while/body/eval_jaxpr/ppermute | solution.py:13
  142.7 3.4 %collective-permute-start = (bf16[256,512]{0,1:T(8,128)(2,1)S(1)}, bf16[256,512]{0,1:T(8,128)(2,1)S(1)}, u32[]{:S(2)}, u32[]{:S(2)}) collective-permute-start(bf16[256,512]{0,1:T(8,128)(2,1)S(1)} %get-tuple-element.288), channel_id=1, source_target_pairs={{0,8},{8,16},{16,24},{1,9},{9,17},{17,25},{2,10},{10,18},{18,26},{... | collective-permute-start | bytes 786440 | tf_op jit(solution)/shard_map/while/body/eval_jaxpr/ppermute | solution.py:13
  148.7 5.1 %fusion.114 = f32[8,256,2,128]{1,0,3,2:T(8,128)S(1)} fusion(f32[8,256,2,128]{1,3,2,0:T(8,128)S(1)} %bitcast.113), kind=kOutput, calls=%fused_computation.9.clone.1 | output fusion | flops 66584576 | bytes 4194304 | tf_op jit(solution)/shard_map/reduce-window.6
  154.6 3.3 %fusion.116 = bf16[8,256,256]{1,2,0:T(8,128)(2,1)S(1)} fusion(f32[8,256,2,128]{1,3,2,0:T(8,128)S(1)} %copy.45, f32[8,256,256]{1,2,0:T(8,128)S(1)} %get-tuple-element.271, f32[8,256]{1,0:T(8,128)S(1)} %get-tuple-element.286, f32[8,256]{1,0:T(8,128)S(1)} %convert_bitcast_fusion.3, u8[256,256]{0,1:T(8,128)(4,1)S(1)} %get-tuple-element.272), kind=kLoop, calls=%fused_computation.5.clone.1 | loop fusion | flops 12582912 | bytes 5324800 | tf_op jit(solution)/shard_map/while/body/eval_jaxpr/convert_element_type | solution.py:30
  158.4 3.0 %collective-permute-start.2 = (bf16[256,512]{0,1:T(8,128)(2,1)S(1)}, bf16[256,512]{0,1:T(8,128)(2,1)S(1)}, u32[]{:S(2)}, u32[]{:S(2)}) collective-permute-start(bf16[256,512]{0,1:T(8,128)(2,1)S(1)} %get-tuple-element.287), channel_id=1, source_target_pairs={{0,8},{8,16},{16,24},{1,9},{9,17},{17,25},{2,10},{10,18},{18,26},{... | collective-permute-start | bytes 786440 | tf_op jit(solution)/shard_map/while/body/eval_jaxpr/ppermute | solution.py:13
  161.4 4.0 %collective-permute-start.1 = (bf16[256,8]{0,1:T(8,128)(2,1)S(1)}, bf16[256,8]{0,1:T(8,128)(2,1)S(1)}, u32[]{:S(2)}, u32[]{:S(2)}) collective-permute-start(bf16[256,8]{0,1:T(8,128)(2,1)S(1)} %get-tuple-element.289), channel_id=1, source_target_pairs={{0,8},{8,16},{16,24},{1,9},{9,17},{17,25},{2,10},{10,18},{18,26},{... | collective-permute-start | bytes 12296 | tf_op jit(solution)/shard_map/while/body/eval_jaxpr/ppermute | solution.py:13
  165.4 4.1 %collective-permute-start = (bf16[256,512]{0,1:T(8,128)(2,1)S(1)}, bf16[256,512]{0,1:T(8,128)(2,1)S(1)}, u32[]{:S(2)}, u32[]{:S(2)}) collective-permute-start(bf16[256,512]{0,1:T(8,128)(2,1)S(1)} %get-tuple-element.288), channel_id=1, source_target_pairs={{0,8},{8,16},{16,24},{1,9},{9,17},{17,25},{2,10},{10,18},{18,26},{... | collective-permute-start | bytes 786440 | tf_op jit(solution)/shard_map/while/body/eval_jaxpr/ppermute | solution.py:13
  172.1 5.1 %fusion.114 = f32[8,256,2,128]{1,0,3,2:T(8,128)S(1)} fusion(f32[8,256,2,128]{1,3,2,0:T(8,128)S(1)} %bitcast.113), kind=kOutput, calls=%fused_computation.9.clone.1 | output fusion | flops 66584576 | bytes 4194304 | tf_op jit(solution)/shard_map/reduce-window.6
  178.0 3.3 %fusion.116 = bf16[8,256,256]{1,2,0:T(8,128)(2,1)S(1)} fusion(f32[8,256,2,128]{1,3,2,0:T(8,128)S(1)} %copy.45, f32[8,256,256]{1,2,0:T(8,128)S(1)} %get-tuple-element.271, f32[8,256]{1,0:T(8,128)S(1)} %get-tuple-element.286, f32[8,256]{1,0:T(8,128)S(1)} %convert_bitcast_fusion.3, u8[256,256]{0,1:T(8,128)(4,1)S(1)} %get-tuple-element.272), kind=kLoop, calls=%fused_computation.5.clone.1 | loop fusion | flops 12582912 | bytes 5324800 | tf_op jit(solution)/shard_map/while/body/eval_jaxpr/convert_element_type | solution.py:30
  183.7 4.3 %collective-permute-start.1 = (bf16[256,8]{0,1:T(8,128)(2,1)S(1)}, bf16[256,8]{0,1:T(8,128)(2,1)S(1)}, u32[]{:S(2)}, u32[]{:S(2)}) collective-permute-start(bf16[256,8]{0,1:T(8,128)(2,1)S(1)} %get-tuple-element.289), channel_id=1, source_target_pairs={{0,8},{8,16},{16,24},{1,9},{9,17},{17,25},{2,10},{10,18},{18,26},{... | collective-permute-start | bytes 12296 | tf_op jit(solution)/shard_map/while/body/eval_jaxpr/ppermute | solution.py:13
  188.0 4.4 %collective-permute-start = (bf16[256,512]{0,1:T(8,128)(2,1)S(1)}, bf16[256,512]{0,1:T(8,128)(2,1)S(1)}, u32[]{:S(2)}, u32[]{:S(2)}) collective-permute-start(bf16[256,512]{0,1:T(8,128)(2,1)S(1)} %get-tuple-element.288), channel_id=1, source_target_pairs={{0,8},{8,16},{16,24},{1,9},{9,17},{17,25},{2,10},{10,18},{18,26},{... | collective-permute-start | bytes 786440 | tf_op jit(solution)/shard_map/while/body/eval_jaxpr/ppermute | solution.py:13
  195.0 5.1 %fusion.114 = f32[8,256,2,128]{1,0,3,2:T(8,128)S(1)} fusion(f32[8,256,2,128]{1,3,2,0:T(8,128)S(1)} %bitcast.113), kind=kOutput, calls=%fused_computation.9.clone.1 | output fusion | flops 66584576 | bytes 4194304 | tf_op jit(solution)/shard_map/reduce-window.6
  201.0 3.3 %fusion.116 = bf16[8,256,256]{1,2,0:T(8,128)(2,1)S(1)} fusion(f32[8,256,2,128]{1,3,2,0:T(8,128)S(1)} %copy.45, f32[8,256,256]{1,2,0:T(8,128)S(1)} %get-tuple-element.271, f32[8,256]{1,0:T(8,128)S(1)} %get-tuple-element.286, f32[8,256]{1,0:T(8,128)S(1)} %convert_bitcast_fusion.3, u8[256,256]{0,1:T(8,128)(4,1)S(1)} %get-tuple-element.272), kind=kLoop, calls=%fused_computation.5.clone.1 | loop fusion | flops 12582912 | bytes 5324800 | tf_op jit(solution)/shard_map/while/body/eval_jaxpr/convert_element_type | solution.py:30
  213.2 30.4 %all-gather.16.cloned.1.call-done = bf16[512,2048]{1,0:T(8,128)(2,1)} async-done(((bf16[512,512]{1,0:T(8,128)(2,1)}), bf16[512,2048]{1,0:T(8,128)(2,1)}) %all-gather.16.cloned.1.call-update) | async-done | bytes 2097168 | tf_op jit(solution)/shard_map/all_gather | solution.py:125
  253.8 26.6 %all-gather.22.cloned.1.call-done = bf16[512,2048]{1,0:T(8,128)(2,1)} async-done(((bf16[512,512]{1,0:T(8,128)(2,1)}), bf16[512,2048]{1,0:T(8,128)(2,1)}) %all-gather.22.cloned.1.call-update) | async-done | bytes 2097168 | tf_op jit(solution)/shard_map/all_gather | solution.py:126
  280.5 3.4 %fusion.13 = bf16[256,2048]{1,0:T(8,128)(2,1)} fusion(f32[256,2048]{1,0:T(8,128)S(1)} %fusion.79, bf16[512,2048]{1,0:T(8,128)(2,1)} %all-gather.22.cloned.1.call-done, f32[256,512]{1,0:T(8,128)S(1)} %get-tuple-element.178, f32[512]{0:T(512)S(1)} %copy-done.6, f32[256]{0:T(256)S(1)} %add_rsqrt_fusion, f32[256]{0:T(256)S(1)} %broadcast_multiply_fusion), kind=kOutput, calls=%fused_computation.28 | convolution fusion | flops 538968064 | bytes 5771264 | tf_op jit(solution)/shard_map/dot_general | solution.py:129
  283.9 8.5 %reduce-scatter.2.cloned.1.call-done = bf16[128,2048]{1,0:T(8,128)(2,1)} async-done(((bf16[256,2048]{1,0:T(8,128)(2,1)}), bf16[128,2048]{1,0:T(8,128)(2,1)}) %reduce-scatter.2.cloned.1.call-update) | async-done | bytes 524304 | tf_op jit(solution)/shard_map/reduce_scatter | solution.py:132
  (115 shorter events, 53.1 us)
Async XLA Ops:
  6.5 14.1 %all-gather.24.cloned.1.call-start = ((), (), s32[]{:S(2)}) async-start(), calls=%async_computation.9 | async-start | bytes 1572864 | tf_op jit(solution)/shard_map/all_gather | solution.py:56
  7.2 4.9 %copy-start.3 = (f32[31,512]{1,0:T(8,128)S(1)}, f32[31,512]{1,0:T(8,128)}, u32[]{:S(2)}) copy-start(f32[31,512]{1,0:T(8,128)} %param.22) | copy-start | bytes 190468
  7.3 51.6 %all-gather.12.cloned.1.call-start = ((), (), s32[]{:S(2)}) async-start(), calls=%async_computation.2 | async-start | bytes 2621440 | tf_op jit(solution)/shard_map/all_gather | solution.py:50
  8.0 50.9 %copy-start.4 = (f32[2048]{0:T(1024)S(1)}, f32[2048]{0:T(1024)}, u32[]{:S(2)}) copy-start(f32[2048]{0:T(1024)} %param.15) | copy-start | bytes 24580
  8.0 87.9 %all-gather.14.cloned.1.call-start = ((), (), s32[]{:S(2)}) async-start(), calls=%async_computation.3 | async-start | bytes 2621440 | tf_op jit(solution)/shard_map/all_gather | solution.py:51
  8.8 124.1 %all-gather.10.cloned.1.call-start = ((), (), s32[]{:S(2)}) async-start(), calls=%async_computation.1 | async-start | bytes 2621440 | tf_op jit(solution)/shard_map/all_gather | solution.py:52
  9.3 195.5 %all-gather.20.cloned.1.call-start = ((), (), s32[]{:S(2)}) async-start(), calls=%async_computation.6 | async-start | bytes 2621440 | tf_op jit(solution)/shard_map/all_gather | solution.py:54
  9.9 197.3 %all-gather.18.cloned.1.call-start = ((), (), s32[]{:S(2)}) async-start(), calls=%async_computation.5 | async-start | bytes 2621440 | tf_op jit(solution)/shard_map/all_gather | solution.py:53
  10.5 233.1 %all-gather.16.cloned.1.call-start = ((), (), s32[]{:S(2)}) async-start(), calls=%async_computation.4 | async-start | bytes 2621440 | tf_op jit(solution)/shard_map/all_gather | solution.py:125
  11.2 269.2 %all-gather.22.cloned.1.call-start = ((), (), s32[]{:S(2)}) async-start(), calls=%async_computation.7 | async-start | bytes 2621440 | tf_op jit(solution)/shard_map/all_gather | solution.py:126
  12.0 280.5 %reduce-scatter.2.cloned.1.call-start = ((), (), s32[]{:S(2)}) async-start(), calls=%async_computation.8 | async-start | bytes 1572864 | tf_op jit(solution)/shard_map/reduce_scatter | solution.py:132
  22.2 73.8 %copy-start = (bf16[1,256,2048]{2,1,0:T(8,128)(2,1)S(1)}, bf16[1,256,2048]{2,1,0:T(8,128)(2,1)}, u32[]{:S(2)}) copy-start(bf16[1,256,2048]{2,1,0:T(8,128)(2,1)} %all-gather.24.cloned.1.call-done) | copy-start | bytes 3145732
  135.7 69.1 %copy-start.5 = (f32[2048]{0:T(1024)S(1)}, f32[2048]{0:T(1024)}, u32[]{:S(2)}) copy-start(f32[2048]{0:T(1024)} %param.15) | copy-start | bytes 24580
  135.9 10.3 %collective-permute-start.2 = (bf16[256,512]{0,1:T(8,128)(2,1)S(1)}, bf16[256,512]{0,1:T(8,128)(2,1)S(1)}, u32[]{:S(2)}, u32[]{:S(2)}) collective-permute-start(bf16[256,512]{0,1:T(8,128)(2,1)S(1)} %get-tuple-element.287), channel_id=1, source_target_pairs={{0,8},{8,16},{16,24},{1,9},{9,17},{17,25},{2,10},{10,18},{18,26},{... | collective-permute-start | bytes 786440 | tf_op jit(solution)/shard_map/while/body/eval_jaxpr/ppermute | solution.py:13
  139.3 6.8 %collective-permute-start.1 = (bf16[256,8]{0,1:T(8,128)(2,1)S(1)}, bf16[256,8]{0,1:T(8,128)(2,1)S(1)}, u32[]{:S(2)}, u32[]{:S(2)}) collective-permute-start(bf16[256,8]{0,1:T(8,128)(2,1)S(1)} %get-tuple-element.289), channel_id=1, source_target_pairs={{0,8},{8,16},{16,24},{1,9},{9,17},{17,25},{2,10},{10,18},{18,26},{... | collective-permute-start | bytes 12296 | tf_op jit(solution)/shard_map/while/body/eval_jaxpr/ppermute | solution.py:13
  142.7 15.3 %collective-permute-start = (bf16[256,512]{0,1:T(8,128)(2,1)S(1)}, bf16[256,512]{0,1:T(8,128)(2,1)S(1)}, u32[]{:S(2)}, u32[]{:S(2)}) collective-permute-start(bf16[256,512]{0,1:T(8,128)(2,1)S(1)} %get-tuple-element.288), channel_id=1, source_target_pairs={{0,8},{8,16},{16,24},{1,9},{9,17},{17,25},{2,10},{10,18},{18,26},{... | collective-permute-start | bytes 786440 | tf_op jit(solution)/shard_map/while/body/eval_jaxpr/ppermute | solution.py:13
  158.4 11.2 %collective-permute-start.2 = (bf16[256,512]{0,1:T(8,128)(2,1)S(1)}, bf16[256,512]{0,1:T(8,128)(2,1)S(1)}, u32[]{:S(2)}, u32[]{:S(2)}) collective-permute-start(bf16[256,512]{0,1:T(8,128)(2,1)S(1)} %get-tuple-element.287), channel_id=1, source_target_pairs={{0,8},{8,16},{16,24},{1,9},{9,17},{17,25},{2,10},{10,18},{18,26},{... | collective-permute-start | bytes 786440 | tf_op jit(solution)/shard_map/while/body/eval_jaxpr/ppermute | solution.py:13
  161.4 8.1 %collective-permute-start.1 = (bf16[256,8]{0,1:T(8,128)(2,1)S(1)}, bf16[256,8]{0,1:T(8,128)(2,1)S(1)}, u32[]{:S(2)}, u32[]{:S(2)}) collective-permute-start(bf16[256,8]{0,1:T(8,128)(2,1)S(1)} %get-tuple-element.289), channel_id=1, source_target_pairs={{0,8},{8,16},{16,24},{1,9},{9,17},{17,25},{2,10},{10,18},{18,26},{... | collective-permute-start | bytes 12296 | tf_op jit(solution)/shard_map/while/body/eval_jaxpr/ppermute | solution.py:13
  165.4 16.0 %collective-permute-start = (bf16[256,512]{0,1:T(8,128)(2,1)S(1)}, bf16[256,512]{0,1:T(8,128)(2,1)S(1)}, u32[]{:S(2)}, u32[]{:S(2)}) collective-permute-start(bf16[256,512]{0,1:T(8,128)(2,1)S(1)} %get-tuple-element.288), channel_id=1, source_target_pairs={{0,8},{8,16},{16,24},{1,9},{9,17},{17,25},{2,10},{10,18},{18,26},{... | collective-permute-start | bytes 786440 | tf_op jit(solution)/shard_map/while/body/eval_jaxpr/ppermute | solution.py:13
  181.8 10.7 %collective-permute-start.2 = (bf16[256,512]{0,1:T(8,128)(2,1)S(1)}, bf16[256,512]{0,1:T(8,128)(2,1)S(1)}, u32[]{:S(2)}, u32[]{:S(2)}) collective-permute-start(bf16[256,512]{0,1:T(8,128)(2,1)S(1)} %get-tuple-element.287), channel_id=1, source_target_pairs={{0,8},{8,16},{16,24},{1,9},{9,17},{17,25},{2,10},{10,18},{18,26},{... | collective-permute-start | bytes 786440 | tf_op jit(solution)/shard_map/while/body/eval_jaxpr/ppermute | solution.py:13
  183.7 8.8 %collective-permute-start.1 = (bf16[256,8]{0,1:T(8,128)(2,1)S(1)}, bf16[256,8]{0,1:T(8,128)(2,1)S(1)}, u32[]{:S(2)}, u32[]{:S(2)}) collective-permute-start(bf16[256,8]{0,1:T(8,128)(2,1)S(1)} %get-tuple-element.289), channel_id=1, source_target_pairs={{0,8},{8,16},{16,24},{1,9},{9,17},{17,25},{2,10},{10,18},{18,26},{... | collective-permute-start | bytes 12296 | tf_op jit(solution)/shard_map/while/body/eval_jaxpr/ppermute | solution.py:13
  188.0 16.3 %collective-permute-start = (bf16[256,512]{0,1:T(8,128)(2,1)S(1)}, bf16[256,512]{0,1:T(8,128)(2,1)S(1)}, u32[]{:S(2)}, u32[]{:S(2)}) collective-permute-start(bf16[256,512]{0,1:T(8,128)(2,1)S(1)} %get-tuple-element.288), channel_id=1, source_target_pairs={{0,8},{8,16},{16,24},{1,9},{9,17},{17,25},{2,10},{10,18},{18,26},{... | collective-permute-start | bytes 786440 | tf_op jit(solution)/shard_map/while/body/eval_jaxpr/ppermute | solution.py:13
  210.3 35.6 %collective-permute-start.3 = (bf16[30,512]{1,0:T(8,128)(2,1)S(1)}, bf16[30,512]{1,0:T(8,128)(2,1)S(1)}, u32[]{:S(2)}, u32[]{:S(2)}) collective-permute-start(bf16[30,512]{1,0:T(8,128)(2,1)S(1)} %slice.274), channel_id=1, source_target_pairs={{0,8},{8,16},{16,24},{1,9},{9,17},{17,25},{2,10},{10,18},{18,26},{... | collective-permute-start | bytes 92168 | tf_op jit(solution)/shard_map/ppermute | solution.py:13
  246.0 34.4 %copy-start.6 = (f32[512]{0:T(512)S(1)}, f32[512]{0:T(512)}, u32[]{:S(2)}) copy-start(f32[512]{0:T(512)} %param.23) | copy-start | bytes 6148
  (2 other events, 3.1 us)
Sparse Core Ops, SparseCore 0:
  8.9 11.7 all-gather.23
  22.5 36.3 all-gather.11
  60.7 35.1 all-gather.13
  97.6 35.1 all-gather.9
  134.5 35.1 all-gather.19
  171.5 35.1 all-gather.17
  208.5 35.0 all-gather.15
  245.4 35.0 all-gather.21
  284.1 8.3 reduce-scatter.1
where the time goes:
time: 300 us; the launch traced here: 299 us
  waiting for transfers between devices  173 us (58%)
  other arithmetic  44.4 us (15%)
  starting transfers between devices  35.1 us (12%)
  matrix products  23.2 us (8%)
  between operations  13.5 us (4%)
  blocking collectives  4.94 us (2%)
  local copies, waits for them, and re-layouts  4.72 us (2%)
    all_gather x1, waiting for transfers between devices, shards(): lax.all_gather(w_query, 'fs', axis=0, tiled=True)  36.7 us
    ppermute x10, starting transfers between devices, shifted(): return lax.ppermute(block, axis, route)  34.8 us
    all_gather x1, waiting for transfers between devices, shards(): lax.all_gather(w_key, 'fs', axis=0, tiled=True)  34.2 us
    all_gather x1, waiting for transfers between devices, shards(): lax.all_gather(w_attn_out, 'fs', axis=1, tiled=True)  30.4 us
    all_gather x1, waiting for transfers between devices, shards(): lax.all_gather(w_conv_out, 'fs', axis=1, tiled=True)  26.6 us
    all_gather x1, waiting for transfers between devices, shards(): lax.all_gather(w_value, 'fs', axis=0, tiled=True)  23.1 us
    another operation x8, other arithmetic  20.5 us
    convert_element_type x4, other arithmetic, piece_terms(): weights.astype(jnp.bfloat16)  12.9 us
  transfers between devices with their start and end apart: 19, of which 7 were waited for; matrix products, arithmetic and copies ran while one was open for 23% of the time, Pallas kernels for 0%

commit v1 on v0

--- a/solution.py
+++ b/solution.py
@@ -1,10 +1,480 @@
+import functools
+
 import jax
 import jax.numpy as jnp
 from jax import lax
+from jax.experimental import pallas as pl
+from jax.experimental.pallas import tpu as pltpu
 from jax.sharding import PartitionSpec as P
 
 HD = 64
 CC = 1024
+MESH = pl.DeviceIdType.MESH
+F32 = jnp.float32
+BF16 = jnp.bfloat16
+
+
+def remote(src, dst, send, recv, **where):
+    return pltpu.make_async_remote_copy(
+        src_ref=src, dst_ref=dst, send_sem=send, recv_sem=recv, device_id=where, device_id_type=MESH
+    )
+
+
+def greet(peers):
+    barrier = pltpu.get_barrier_semaphore()
+    for where in peers:
+        pl.semaphore_signal(barrier, inc=1, device_id=where, device_id_type=MESH)
+    pl.semaphore_wait(barrier, len(peers))
+
+
+def plane(fs):
+    y = (fs + 2) % 4
+    return fs + 1 - 2 * (fs % 2), y, y + 1 - 2 * (y % 2)
+
+
+class OutGather:
+    def __init__(self, sources, targets, sems):
+        self.sources, self.targets = sources, targets
+        self.send, self.recv, self.psend, self.precv, self.local = sems
+        self.fs, self.tp = lax.axis_index("fs"), lax.axis_index("tp")
+
+    def slot(self, k, owner, group):
+        rows, cols = self.sources[k].shape
+        return self.targets[k].at[
+            pl.ds(pl.multiple_of(group * rows, rows), rows),
+            pl.ds(pl.multiple_of(owner * cols, cols), cols),
+        ]
+
+    def hop(self, src, k, owner, sem, to):
+        return remote(src, self.slot(k, owner, self.tp), self.send.at[sem], self.recv.at[sem], fs=to)
+
+    def other(self, src, k, owner, sem):
+        return remote(
+            src, self.slot(k, owner, self.tp), self.psend.at[sem], self.precv.at[sem], tp=1 - self.tp
+        )
+
+    def plan(self):
+        fs = self.fs
+        xn, yn, dg = plane(fs)
+        a, c = self.sources
+        self.first = [
+            self.hop(a, 0, fs, 0, xn), self.hop(c, 1, fs, 1, yn),
+            self.hop(c, 1, fs, 2, xn), self.hop(a, 0, fs, 3, yn),
+        ]
+        self.relay = [
+            self.hop(self.slot(0, xn, self.tp), 0, xn, 4, yn),
+            self.hop(self.slot(1, yn, self.tp), 1, yn, 5, xn),
+        ]
+        arrivals = [(0, 0, xn), (1, 1, yn), (2, 1, xn), (3, 0, yn), (4, 0, dg), (5, 1, dg)]
+        self.got = [
+            (self.hop(self.slot(k, o, self.tp), k, o, s, xn), self.other(self.slot(k, o, self.tp), k, o, s))
+            for s, k, o in arrivals
+        ]
+        self.own = [self.other(a, 0, fs, 6), self.other(c, 1, fs, 7)]
+        self.keep = [
+            pltpu.make_async_copy(self.sources[k], self.slot(k, fs, self.tp), self.local.at[k]) for k in (0, 1)
+        ]
+
+    def start(self):
+        self.plan()
+        for copy in self.first + self.own + self.keep:
+            copy.start()
+
+    def middle(self):
+        for s in range(4):
+            arrived, onward = self.got[s]
+            arrived.wait_recv()
+            if s < 2:
+                self.relay[s].start()
+            onward.start()
+
+    def finish(self):
+        for s in (4, 5):
+            arrived, onward = self.got[s]
+            arrived.wait_recv()
+            onward.start()
+        for copy in self.first + self.relay:
+            copy.wait_send()
+        for _, onward in self.got:
+            onward.wait()
+        for copy in self.own:
+            copy.wait()
+        for copy in self.keep:
+            copy.wait()
+
+
+OUT_SEMS = [
+    pltpu.SemaphoreType.DMA((6,)),
+    pltpu.SemaphoreType.DMA((6,)),
+    pltpu.SemaphoreType.DMA((8,)),
+    pltpu.SemaphoreType.DMA((8,)),
+    pltpu.SemaphoreType.DMA((2,)),
+]
+
+
+def gather_kernel(n_sp, with_out, *refs):
+    tok, w_ins, off = refs[0], refs[1:6], refs[6]
+    refs = refs[7:]
+    if with_out:
+        out_sources, refs = refs[:2], refs[2:]
+    tok_all, w_all, off_all = refs[:3]
+    refs = refs[3:]
+    if with_out:
+        out_targets, refs = refs[:2], refs[2:]
+    stage, up_s, up_r, dn_s, dn_r, par_s, par_r, w_s, w_r, off_s, off_r, loc = refs[:12]
+    z, fs, tp = lax.axis_index("sp"), lax.axis_index("fs"), lax.axis_index("tp")
+    xn, yn, dg = plane(fs)
+    rows = w_ins[0].shape[0]
+    width = stage.shape[1] // 5
+    half = rows // 2
+
+    fills = [
+        pltpu.make_async_copy(
+            w.at[:, pl.ds(pl.multiple_of(z * width, width), width)],
+            stage.at[:, pl.ds(k * width, width)],
+            loc.at[k],
+        )
+        for k, w in enumerate(w_ins)
+    ]
+    for fill in fills:
+        fill.start()
+    keep_tok = pltpu.make_async_copy(tok, tok_all.at[z, tp], loc.at[5])
+    keep_off = pltpu.make_async_copy(off, off_all.at[z], loc.at[6])
+    keep_tok.start()
+    keep_off.start()
+    greet(
+        [{"sp": (z + d) % n_sp} for d in range(1, n_sp)]
+        + [{"fs": xn}, {"fs": yn}, {"tp": 1 - tp}]
+    )
+
+    def lift(src, block, dist):
+        return remote(src, tok_all.at[block, tp], up_s.at[dist - 1], up_r.at[dist - 1], sp=(z + 1) % n_sp)
+
+    def sink(src, block, dist):
+        return remote(src, tok_all.at[block, tp], dn_s.at[dist - 1], dn_r.at[dist - 1], sp=(z + n_sp - 1) % n_sp)
+
+    def across(src, block):
+        return remote(src, tok_all.at[block, tp], par_s.at[block], par_r.at[block], tp=1 - tp)
+
+    @pl.when(z < n_sp - 1)
+    def _():
+        lift(tok, z, 1).start()
+
+    @pl.when(z > 0)
+    def _():
+        sink(tok, z, 1).start()
+
+    across(tok, z).start()
+    offs = [
+        remote(off, off_all.at[z], off_s.at[d - 1], off_r.at[d - 1], sp=(z + d) % n_sp) for d in range(1, n_sp)
+    ]
+    for copy in offs:
+        copy.start()
+    for fill in fills:
+        fill.wait()
+    keep_w = pltpu.make_async_copy(stage, w_all.at[pl.ds(pl.multiple_of(fs * rows, rows), rows)], loc.at[7])
+    keep_w.start()
+
+    def part(owner, h):
+        return w_all.at[pl.ds(pl.multiple_of(owner * rows + h * half, half), half)]
+
+    def send_w(src, owner, h, sem, to):
+        return remote(src, part(owner, h), w_s.at[sem], w_r.at[sem], fs=to)
+
+    own = [stage.at[pl.ds(h * half, half)] for h in range(2)]
+    first = [
+        send_w(own[0], fs, 0, 0, xn), send_w(own[1], fs, 1, 1, yn),
+        send_w(own[1], fs, 1, 2, xn), send_w(own[0], fs, 0, 3, yn),
+    ]
+    for copy in first:
+        copy.start()
+    relay = [send_w(part(xn, 0), xn, 0, 4, yn), send_w(part(yn, 1), yn, 1, 5, xn)]
+    if with_out:
+        gather = OutGather(out_sources, out_targets, refs[12:])
+    arrivals = [(0, xn, 0), (1, yn, 1), (2, xn, 1), (3, yn, 0), (4, dg, 0), (5, dg, 1)]
+    for s, owner, h in arrivals[:2]:
+        send_w(part(owner, h), owner, h, s, xn).wait_recv()
+        relay[s].start()
+    if with_out:
+        gather.start()
+
+    for dist in range(1, n_sp):
+        @pl.when(z >= dist)
+        def _():
+            block = (z - dist + n_sp) % n_sp
+            lift(tok_all.at[block, tp], block, dist).wait_recv()
+            if dist < n_sp - 1:
+                @pl.when(z < n_sp - 1)
+                def _():
+                    lift(tok_all.at[block, tp], block, dist + 1).start()
+            across(tok_all.at[block, tp], block).start()
+
+        @pl.when(z + dist < n_sp)
+        def _():
+            block = (z + dist) % n_sp
+            sink(tok_all.at[block, tp], block, dist).wait_recv()
+            if dist < n_sp - 1:
+                @pl.when(z > 0)
+                def _():
+                    sink(tok_all.at[block, tp], block, dist + 1).start()
+            across(tok_all.at[block, tp], block).start()
+
+    for s, owner, h in arrivals[2:]:
+        send_w(part(owner, h), owner, h, s, xn).wait_recv()
+    if with_out:
+        gather.middle()
+        gather.finish()
+    for copy in first + relay:
+        copy.wait_send()
+    for dist in range(1, n_sp):
+        @pl.when(jnp.logical_and(z < n_sp - 1, z >= dist - 1))
+        def _():
+            lift(tok, z, dist).wait_send()
+
+        @pl.when(jnp.logical_and(z > 0, z + dist - 1 < n_sp))
+        def _():
+            sink(tok, z, dist).wait_send()
+
+    for block in range(n_sp):
+        remote(tok, tok_all.at[block, 1 - tp], par_s.at[block], par_r.at[block], tp=1 - tp).wait()
+    for copy in offs:
+        copy.wait()
+    keep_tok.wait()
+    keep_off.wait()
+    keep_w.wait()
+
+
+ANY = pl.BlockSpec(memory_space=pl.ANY)
+VMEM = pl.BlockSpec(memory_space=pltpu.VMEM)
+
+
+def gather_call(n_sp, n_fs, n_tp, width, tokens, w_ins, offsets, w_outs):
+    rows, features = tokens.shape
+    depth = w_ins[0].shape[0]
+    o_rows, o_cols = w_outs[0].shape
+    dma = pltpu.SemaphoreType.DMA
+    return pl.pallas_call(
+        functools.partial(gather_kernel, n_sp, True),
+        out_shape=[
+            jax.ShapeDtypeStruct((n_sp, n_tp, rows, features), BF16),
+            jax.ShapeDtypeStruct((n_fs * depth, 5 * width), BF16),
+            jax.ShapeDtypeStruct((n_sp,) + offsets.shape, F32),
+            jax.ShapeDtypeStruct((n_tp * o_rows, n_fs * o_cols), BF16),
+            jax.ShapeDtypeStruct((n_tp * o_rows, n_fs * o_cols), BF16),
+        ],
+        in_specs=[ANY] * 9,
+        out_specs=[ANY] * 5,
+        scratch_shapes=[
+            pltpu.VMEM((depth, 5 * width), BF16),
+            dma((n_sp - 1,)), dma((n_sp - 1,)), dma((n_sp - 1,)), dma((n_sp - 1,)),
+            dma((n_sp,)), dma((n_sp,)),
+            dma((6,)), dma((6,)),
+            dma((n_sp - 1,)), dma((n_sp - 1,)),
+            dma((8,)),
+        ] + OUT_SEMS,
+        compiler_params=pltpu.CompilerParams(collective_id=0, has_side_effects=True),
+        name="gather_inputs",
+    )(tokens, *w_ins, offsets, *w_outs)
+
+
+def compute_body(width, heads, taps, blk, tok, gain, w, off, ck, attn_out, conv_out, mean_out, proj, gated):
+    length = tok.shape[0]
+    n_rows = mean_out.shape[2]
+
+    def project(i, _):
+        at = pl.ds(pl.multiple_of(i * 128, 128), 128)
+        x = tok[at, :].astype(F32)
+        normed = (x * lax.rsqrt(jnp.mean(x * x, axis=1, keepdims=True) + 1e-06) * gain[...]).astype(BF16)
+        out = jnp.dot(normed, w[...], preferred_element_type=F32).astype(BF16)
+        proj[at, :] = out[:, : 3 * width]
+        value = out[:, 3 * width : 4 * width].astype(F32)
+        gate = out[:, 4 * width :].astype(F32)
+        gated[pl.ds(pl.multiple_of(i * 128 + 32, 32), 128), :] = (value * jax.nn.sigmoid(gate)).astype(BF16).astype(F32)
+        return 0
+
+    gated[pl.ds(0, 32), :] = jnp.zeros((32, width), F32)
+    lax.fori_loop(0, length // 128, project, 0)
+
+    ones = jnp.full((8, width), 1.0 / width, F32)
+
+    def convolve(i, _):
+        base = pl.multiple_of(i * n_rows, n_rows)
+        window = gated[pl.ds(base, n_rows + 32), :]
+        total = jnp.zeros((n_rows, width), F32)
+        for tap in range(taps):
+            lo = 32 - (taps - 1) + tap
+            total = total + ck[tap : tap + 1, :] * window[lo : lo + n_rows]
+        local = jnp.mean(total, axis=1, keepdims=True)
+        conv_out[pl.ds(base, n_rows), :] = (total - local).astype(BF16)
+        mean_out[i] = lax.dot_general(
+            ones, total, (((1,), (1,)), ((), ())), precision=lax.Precision.HIGHEST, preferred_element_type=F32
+        )
+        return 0
+
+    lax.fori_loop(0, length // n_rows, convolve, 0)
+
+    row = lax.broadcasted_iota(jnp.int32, (blk, blk), 0)
+    col = lax.broadcasted_iota(jnp.int32, (blk, blk), 1)
+    allowed = col < row
+    after = jnp.where(row >= col, 1.0, 0.0).astype(BF16)
+    lane = lax.broadcasted_iota(jnp.int32, (blk, width), 1)
+
+    def attend(i, _):
+        q_at = pl.ds(pl.multiple_of(i * blk, blk), blk)
+        merged = jnp.zeros((blk, width), F32)
+        for h in range(heads):
+            mine = jnp.logical_and(lane >= h * HD, lane < (h + 1) * HD)
+            q = jnp.where(mine, proj[q_at, :width].astype(F32) * HD ** (-0.5), 0.0).astype(BF16)
+
+            def piece(j, carry, total, diagonal):
+                k_at = pl.ds(pl.multiple_of(j * blk, blk), blk)
+                k = proj[k_at, width : 2 * width]
+                v = proj[k_at, 2 * width : 3 * width]
+                s = lax.dot_general(q, k, (((1,), (1,)), ((), ())), preferred_element_type=F32)
+                s = s + off[j, h : h + 1, :]
+                keep = -(jnp.maximum(s, 0.0) + jnp.log(1.0 + jnp.exp(-jnp.abs(s))))
+                if diagonal:
+                    keep = jnp.where(allowed, keep, 0.0)
+                high = keep.astype(BF16)
+                low = (keep - high.astype(F32)).astype(BF16)
+                suffix = jnp.dot(high, after, preferred_element_type=F32)
+                suffix = suffix + jnp.dot(low, after, preferred_element_type=F32)
+                weights = jnp.exp(s + suffix + carry)
+                if diagonal:
+                    weights = jnp.where(allowed, weights, 0.0)
+                total = total + jnp.dot(weights.astype(BF16), v, preferred_element_type=F32)
+                return carry + suffix[:, :1], total
+
+            carry, total = piece(i, jnp.zeros((blk, 1), F32), jnp.zeros((blk, width), F32), True)
+            carry, total = lax.fori_loop(
+                0, i, lambda t, c: piece(i - 1 - t, c[0], c[1], False), (carry, total)
+            )
+            merged = jnp.where(mine, total, merged)
+        attn_out[q_at, :] = merged.astype(BF16)
+        return 0
+
+    lax.fori_loop(0, length // blk, attend, 0)
+
+
+def compute_call(width, heads, blk, n_dest, tok, gain, w, off, ck):
+    length = tok.shape[0]
+    return pl.pallas_call(
+        functools.partial(compute_body, width, heads, ck.shape[0], blk),
+        out_shape=[
+            jax.ShapeDtypeStruct((length, width), BF16),
+            jax.ShapeDtypeStruct((length, width), BF16),
+            jax.ShapeDtypeStruct((n_dest, 8, length // n_dest), F32),
+        ],
+        in_specs=[VMEM] * 5,
+        out_specs=[VMEM] * 3,
+        scratch_shapes=[pltpu.VMEM((length, 3 * width), BF16), pltpu.VMEM((length + 32, width), F32)],
+        name="branches",
+    )(tok, gain, w, off, ck)
+
+
+def exchange_kernel(n_sp, n_tp, attn, conv, mean, x_out, mean_all, send, recv, loc):
+    z, tp = lax.axis_index("sp"), lax.axis_index("tp")
+    me = z * n_tp + tp
+    n = n_sp * n_tp
+    rows, cols = x_out.shape
+    width = attn.shape[1]
+    place = tp * n_sp + z
+
+    def slots(index):
+        return (
+            x_out.at[:, pl.ds(pl.multiple_of(index * width, width), width)],
+            x_out.at[:, pl.ds(pl.multiple_of(cols // 2 + index * width, width), width)],
+            mean_all.at[index],
+        )
+
+    def pieces(dest):
+        at = pl.ds(pl.multiple_of(dest * rows, rows), rows)
+        return (attn.at[at], conv.at[at], mean.at[dest])
+
+    keeps = [
+        pltpu.make_async_copy(s, d, loc.at[k]) for k, (s, d) in enumerate(zip(pieces(me), slots(place)))
+    ]
+    for copy in keeps:
+        copy.start()
+    peers = [(me + d) % n for d in range(1, n)]
+    greet([{"sp": p // n_tp, "tp": p % n_tp} for p in peers])
+    copies = []
+    for d, p in enumerate(peers):
+        for k, (s, t) in enumerate(zip(pieces(p), slots(place))):
+            copies.append(remote(s, t, send.at[d, k], recv.at[d, k], sp=p // n_tp, tp=p % n_tp))
+    for copy in copies:
+        copy.start()
+    for d in range(1, n):
+        src = (me - d + n) % n
+        for k, (s, t) in enumerate(zip(pieces(me), slots((src % n_tp) * n_sp + src // n_tp))):
+            remote(s, t, send.at[d - 1, k], recv.at[d - 1, k], sp=z, tp=1 - tp).wait_recv()
+    for copy in copies:
+        copy.wait_send()
+    for copy in keeps:
+        copy.wait()
+
+
+def exchange_call(n_sp, n_tp, attn, conv, mean):
+    n = n_sp * n_tp
+    length, width = attn.shape
+    dma = pltpu.SemaphoreType.DMA
+    return pl.pallas_call(
+        functools.partial(exchange_kernel, n_sp, n_tp),
+        out_shape=[
+            jax.ShapeDtypeStruct((length // n, 2 * width * n), BF16),
+            jax.ShapeDtypeStruct((n, 8, length // n), F32),
+        ],
+        in_specs=[VMEM] * 3,
+        out_specs=[VMEM] * 2,
+        scratch_shapes=[dma((n - 1, 3)), dma((n - 1, 3)), dma((3,))],
+        compiler_params=pltpu.CompilerParams(collective_id=1, has_side_effects=True),
+        name="to_positions",
+    )(attn, conv, mean)
+
+
+def spread_shards(
+    tokens,
+    norm_gain,
+    w_query,
+    w_key,
+    w_value,
+    w_conv_value,
+    w_conv_gate,
+    key_offset,
+    conv_kernel,
+    conv_gain,
+    w_attn_out,
+    w_conv_out,
+):
+    n_sp, n_fs, n_tp = (lax.axis_size(a) for a in ("sp", "fs", "tp"))
+    z, tp = lax.axis_index("sp"), lax.axis_index("tp")
+    width = w_query.shape[1] // n_sp
+    heads = width // HD
+    offsets = jnp.transpose(key_offset.astype(F32))
+    tok_all, w_all, off_all, wa, wc = gather_call(
+        n_sp, n_fs, n_tp, width, tokens[0],
+        (w_query, w_key, w_value, w_conv_value, w_conv_gate), offsets, (w_attn_out, w_conv_out),
+    )
+    features = tokens.shape[2]
+    tok_all = tok_all.reshape(-1, features)
+    off = lax.dynamic_slice_in_dim(off_all, z * heads, heads, axis=1)
+    taps = lax.dynamic_slice_in_dim(conv_kernel, z * width, width, axis=1)
+    attn, conv, mean = compute_call(
+        width, heads, key_offset.shape[0], n_sp * n_tp, tok_all, norm_gain[None], w_all, off, taps
+    )
+    x, means = exchange_call(n_sp, n_tp, attn, conv, mean)
+    half = x.shape[1] // 2
+    groups = n_sp * n_tp
+    local = jnp.transpose(means[:, 0, :])
+    local = local - jnp.mean(local, axis=1, keepdims=True)
+    gain = lax.all_gather(conv_gain, "tp", axis=0, tiled=True)
+    centred = (x[:, half:].astype(F32).reshape(-1, groups, width) + local[:, :, None]).reshape(-1, half)
+    centred = centred - jnp.mean(centred, axis=1, keepdims=True)
+    spread = jnp.mean(centred * centred, axis=1, keepdims=True)
+    hidden = jax.nn.silu(centred * lax.rsqrt(spread + 1e-06) * gain).astype(BF16)
+    mixed = jnp.dot(x[:, :half], wa, preferred_element_type=F32)
+    mixed = mixed + jnp.dot(hidden, wc, preferred_element_type=F32)
+    return mixed.astype(BF16)[None]
 
 
 def shifted(block, axis, distance):
@@ -155,6 +625,21 @@
         P("tp", "fs"),
         P("tp", "fs"),
     )
-    return jax.shard_map(
-        shards, mesh=mesh, in_specs=placed, out_specs=P("fs", ("sp", "tp"), None), check_vma=False
-    )
+
+    def fits(tokens, norm_gain, w_query, *rest):
+        n_sp, n_fs, n_tp = mesh.shape["sp"], mesh.shape["fs"], mesh.shape["tp"]
+        cols = w_query.shape[1] // n_tp
+        return n_fs == 4 and n_tp == 2 and n_sp > 1 and rest[5].shape[0] <= 33 and cols % (128 * n_sp) == 0 and rest[2].shape[1] == w_query.shape[1] and (
+            tokens.shape[1] % (128 * n_sp * n_tp) == 0
+        )
+
+    def program(*args):
+        body = spread_shards if fits(*args) else shards
+        return mapped(body)(*args)
+
+    def mapped(body):
+        return jax.shard_map(
+            body, mesh=mesh, in_specs=placed, out_specs=P("fs", ("sp", "tp"), None), check_vma=False
+        )
+
+    return program

time: 300 us -> 121 us (0.40)
  waiting for transfers between devices: 173 us -> 0 us
  Pallas kernels: 0 us -> 106 us
  other arithmetic: 44.4 us -> 4.63 us
  starting transfers between devices: 35.1 us -> 0 us
  matrix products: 23.2 us -> 4.73 us
  between operations: 13.5 us -> 0.05 us
    all_gather x8 -> x0, waiting for transfers between devices: 160 us -> none  [the longest x1 36.7 us: shards(): lax.all_gather(w_query, 'fs', axis=0, tiled=True)]
    pallas_call x0 -> x3, Pallas kernels: none -> 106 us  [the longest x1 65.2 us: gather_call(): pl.pallas_call(functools.partial(gather_kernel, n_sp, True), out_shape=[j...]
    ppermute x10 -> x0, starting transfers between devices: 34.8 us -> none  [shifted(): return lax.ppermute(block, axis, route)]
    another operation x12 -> x0, other arithmetic: 21 us -> none
    dot_general x15 -> x2, matrix products: 23.2 us -> 4.73 us  [the longest x1 3 us: spread_shards(): mixed = jnp.dot(x[:, :half], wa, preferred_element_type=F32)]
    convert_element_type x6 -> x0, other arithmetic: 13 us -> none  [the longest x4 12.9 us: piece_terms(): weights.astype(jnp.bfloat16)]
    reduce_scatter x1 -> x0, waiting for transfers between devices: 8.52 us -> none  [shards(): lax.psum_scatter(lax.optimization_barrier(partial_value.astype(jnp.bfloat...]
    reduce_sum x7 -> x3, other arithmetic: 10.3 us -> 3.28 us  [the longest x1 1.27 us: spread_shards(): centred = centred - jnp.mean(centred, axis=1, keepdims=True)]
  transfers between devices with their start and end apart: 19 -> 0, of which waited for: 7 -> 0; matrix products, arithmetic and copies ran while one was open for 23% -> 0% of each run, Pallas kernels for 0% -> 0%
where the time goes in v1:
time: 121 us; the launch traced here: 120 us
  Pallas kernels  106 us (88%)
  matrix products  4.73 us (4%)
  other arithmetic  4.63 us (4%)
  blocking collectives  2.8 us (2%)
  local copies, waits for them, and re-layouts  2.28 us (2%)
    pallas_call x1, Pallas kernels, gather_call(): pl.pallas_call(functools.partial(gather_kernel, n_sp, True), out_shape=[j...  65.2 us
    pallas_call x1, Pallas kernels, compute_call(): pl.pallas_call(functools.partial(compute_body, width, heads, ck.shape[0],...  25.9 us
    pallas_call x1, Pallas kernels, exchange_call(): pl.pallas_call(functools.partial(exchange_kernel, n_sp, n_tp), out_shape=...  14.4 us
    dot_general x1, matrix products, spread_shards(): mixed = jnp.dot(x[:, :half], wa, preferred_element_type=F32)  3 us
    all_gather x1, blocking collectives, spread_shards(): gain = lax.all_gather(conv_gain, 'tp', axis=0, tiled=True)  2.8 us

profile of v1, /device:TPU:0, one launch (start us, length us, event | category | flops | bytes accessed | tf_op | source)
XLA Modules:
  0.0 120.1 jit_solution(16358849297887800142)
XLA Ops:
  0.0 0.0 copy-start
  0.0 1.3 %convert_bitcast_fusion.refs_6_ = f32[8,256]{1,0:T(8,128)} fusion(bf16[256,8]{0,1:T(8,128)(2,1)} %param.19), kind=kLoop, calls=%fused_computation.13 | loop fusion | flops 2048 | bytes 12288 | tf_op jit(solution)/shard_map/transpose | solution.py:453
  1.3 65.2 %gather_inputs.1 = (bf16[4,2,128,2048]{3,2,1,0:T(8,128)(2,1)}, bf16[2048,640]{1,0:T(8,128)(2,1)}, f32[4,8,256]{2,1,0:T(8,128)}, bf16[1024,2048]{1,0:T(8,128)(2,1)}, bf16[1024,2048]{1,0:T(8,128)(2,1)}) custom-call(bf16[128,2048]{1,0:T(8,128)(2,1)} %bitcast.28, bf16[512,512]{1,0:T(8,128)(2,1)} %refs_1_.1, bf16[512,512]{1,0:T(8,128)(2,1)} %refs_2_.1, ...), custom_call_target="tpu_custom_call" | custom-call | tf_op jit(solution)/shard_map/gather_inputs/pallas_call | solution.py:256
  66.6 1.4 %constant_dynamic-slice_fusion.1.off = f32[4,2,256]{2,1,0:T(2,128)} fusion(f32[4,8,256]{2,1,0:T(8,128)} %get-tuple-element.17, s32[]{:T(128)S(6)} %select_n.6), kind=kLoop, calls=%fused_computation.17 | loop fusion | bytes 16388 | tf_op jit(solution)/shard_map/dynamic_slice | solution.py:460
  67.9 0.0 copy-done
  67.9 0.6 constant_dynamic-slice_fusion.ck
  68.5 25.9 %branches.1 = (bf16[1024,128]{1,0:T(8,128)(2,1)}, bf16[1024,128]{1,0:T(8,128)(2,1)}, f32[8,8,128]{2,1,0:T(8,128)}) custom-call(bf16[1024,2048]{1,0:T(8,128)(2,1)} %bitcast.27, f32[1,2048]{1,0:T(1,128)} %bitcast.30, bf16[2048,640]{1,0:T(8,128)(2,1)} %get-tuple-element.16.w, f32[4,2,256]{2,1,0:T(2,128)} %constant_dynamic-slice_fusion.1.off, ...), custom_call_target="tpu_custom_call" | custom-call | tf_op jit(solution)/shard_map/branches/pallas_call | solution.py:361
  94.4 0.0 copy-start.2
  94.4 14.4 %to_positions.1 = (bf16[128,2048]{1,0:T(8,128)(2,1)}, f32[8,8,128]{2,1,0:T(8,128)}) custom-call(bf16[1024,128]{1,0:T(8,128)(2,1)} %get-tuple-element.18.attn, bf16[1024,128]{1,0:T(8,128)(2,1)} %get-tuple-element.19.conv, f32[8,8,128]{2,1,0:T(8,128)} %get-tuple-element.20.mean), custom_call_target="tpu_custom_call" | custom-call | tf_op jit(solution)/shard_map/to_positions/pallas_call | solution.py:421
  108.9 0.0 copy-start.1
  108.9 0.8 slice_reduce_fusion
  109.7 0.1 copy.14
  109.8 0.0 copy-start.3
  109.9 0.2 add.37
  110.0 1.3 %fusion.8 = f32[128]{0:T(128)S(1)} fusion(f32[16,8,8,128]{3,2,1,0:T(8,128)S(1)} %bitcast.24, bf16[128,2048]{1,0:T(8,128)(2,1)} %get-tuple-element.21), kind=kLoop, calls=%fused_computation.12 | loop fusion | flops 393088 | bytes 786944 | tf_op jit(solution)/shard_map/reduce_sum | solution.py:472
  111.3 1.2 multiply_reduce_fusion
  112.5 3.0 %fusion.6 = f32[128,2048]{1,0:T(8,128)S(1)} fusion(bf16[1024,2048]{1,0:T(8,128)(2,1)} %get-tuple-element.22, bf16[128,2048]{1,0:T(8,128)(2,1)} %get-tuple-element.21), kind=kOutput, calls=%fused_computation.10 | convolution fusion | flops 536870912 | bytes 5505024 | tf_op jit(solution)/shard_map/dot_general | solution.py:475
  115.5 0.0 copy-done.2
  115.5 2.8 %all-gather = f32[2,1,512]{2,1,0:T(1,128)S(1)} all-gather(f32[1,1,512]{2,1,0:T(1,128)S(1)} %bitcast.32), channel_id=1, replica_groups=mesh['sp'=4,'fs'=4,'tp'=2] {'tp'}, dimensions={0}, use_global_device_ids=true | all-gather | bytes 6144 | tf_op jit(solution)/shard_map/all_gather | solution.py:470
  118.3 0.0 copy-done.1
  118.3 0.0 copy-done.3
  118.3 1.7 %fusion.1 = bf16[1,128,2048]{2,1,0:T(8,128)(2,1)} fusion(f32[128,2048]{1,0:T(8,128)S(1)} %fusion.6, bf16[1024,2048]{1,0:T(8,128)(2,1)S(1)} %copy-done.3, f32[1024]{0:T(1024)S(1)} %bitcast.31, f32[128]{0:T(128)S(1)} %add_rsqrt_fusion, f32[128]{0:T(128)S(1)} %broadcast_multiply_fusion, f32[16,8,8,128]{3,2,1,0:T(8,128)S(1)} %bitcast.26, ...), kind=kOutput, calls=%fused_computation.2 | convolution fusion | flops 538705920 | bytes 6558720 | tf_op jit(solution)/shard_map/dot_general | solution.py:476
  (4 shorter events, 0.0 us)
Async XLA Ops:
  0.0 67.9 %copy-start = (f32[31,512]{1,0:T(8,128)S(1)}, f32[31,512]{1,0:T(8,128)}, u32[]{:S(2)}) copy-start(f32[31,512]{1,0:T(8,128)} %param.20) | copy-start | bytes 190468
  94.4 21.1 %copy-start.2 = (f32[512]{0:T(512)S(1)}, f32[512]{0:T(512)}, u32[]{:S(2)}) copy-start(f32[512]{0:T(512)} %param.21) | copy-start | bytes 6148
  108.9 9.4 %copy-start.1 = (bf16[128,2048]{1,0:T(8,128)(2,1)S(1)}, bf16[128,2048]{1,0:T(8,128)(2,1)}, u32[]{:S(2)}) copy-start(bf16[128,2048]{1,0:T(8,128)(2,1)} %get-tuple-element.21) | copy-start | bytes 1572868
  109.8 8.5 %copy-start.3 = (bf16[1024,2048]{1,0:T(8,128)(2,1)S(1)}, bf16[1024,2048]{1,0:T(8,128)(2,1)}, u32[]{:S(2)}) copy-start(bf16[1024,2048]{1,0:T(8,128)(2,1)} %get-tuple-element.24) | copy-start | bytes 12582916

commit v2 on v1

--- a/solution.py
+++ b/solution.py
@@ -33,15 +33,17 @@
 
 
 class OutGather:
-    def __init__(self, sources, targets, sems):
-        self.sources, self.targets = sources, targets
+    def __init__(self, source, target, sems):
+        half = source.shape[0] // 2
+        self.sources = [source.at[pl.ds(k * half, half)] for k in range(2)]
+        self.target = target
         self.send, self.recv, self.psend, self.precv, self.local = sems
         self.fs, self.tp = lax.axis_index("fs"), lax.axis_index("tp")
 
     def slot(self, k, owner, group):
         rows, cols = self.sources[k].shape
-        return self.targets[k].at[
-            pl.ds(pl.multiple_of(group * rows, rows), rows),
+        return self.target.at[
+            pl.ds(pl.multiple_of((group * 2 + k) * rows, rows), rows),
             pl.ds(pl.multiple_of(owner * cols, cols), cols),
         ]
 
@@ -116,11 +118,11 @@
     tok, w_ins, off = refs[0], refs[1:6], refs[6]
     refs = refs[7:]
     if with_out:
-        out_sources, refs = refs[:2], refs[2:]
+        out_source, cgain, refs = refs[0], refs[1], refs[2:]
     tok_all, w_all, off_all = refs[:3]
     refs = refs[3:]
     if with_out:
-        out_targets, refs = refs[:2], refs[2:]
+        out_target, cgain_all, refs = refs[0], refs[1], refs[2:]
     stage, up_s, up_r, dn_s, dn_r, par_s, par_r, w_s, w_r, off_s, off_r, loc = refs[:12]
     z, fs, tp = lax.axis_index("sp"), lax.axis_index("fs"), lax.axis_index("tp")
     xn, yn, dg = plane(fs)
@@ -140,8 +142,10 @@
         fill.start()
     keep_tok = pltpu.make_async_copy(tok, tok_all.at[z, tp], loc.at[5])
     keep_off = pltpu.make_async_copy(off, off_all.at[z], loc.at[6])
+    keep_gain = pltpu.make_async_copy(cgain, cgain_all.at[tp], loc.at[8])
     keep_tok.start()
     keep_off.start()
+    keep_gain.start()
     greet(
         [{"sp": (z + d) % n_sp} for d in range(1, n_sp)]
         + [{"fs": xn}, {"fs": yn}, {"tp": 1 - tp}]
@@ -168,6 +172,8 @@
     offs = [
         remote(off, off_all.at[z], off_s.at[d - 1], off_r.at[d - 1], sp=(z + d) % n_sp) for d in range(1, n_sp)
     ]
+    gain_copy = remote(cgain, cgain_all.at[tp], refs[17].at[0], refs[17].at[1], tp=1 - tp)
+    gain_copy.start()
     for copy in offs:
         copy.start()
     for fill in fills:
@@ -190,7 +196,7 @@
         copy.start()
     relay = [send_w(part(xn, 0), xn, 0, 4, yn), send_w(part(yn, 1), yn, 1, 5, xn)]
     if with_out:
-        gather = OutGather(out_sources, out_targets, refs[12:])
+        gather = OutGather(out_source, out_target, refs[12:17])
     arrivals = [(0, xn, 0), (1, yn, 1), (2, xn, 1), (3, yn, 0), (4, dg, 0), (5, dg, 1)]
     for s, owner, h in arrivals[:2]:
         send_w(part(owner, h), owner, h, s, xn).wait_recv()
@@ -239,6 +245,8 @@
         remote(tok, tok_all.at[block, 1 - tp], par_s.at[block], par_r.at[block], tp=1 - tp).wait()
     for copy in offs:
         copy.wait()
+    gain_copy.wait()
+    keep_gain.wait()
     keep_tok.wait()
     keep_off.wait()
     keep_w.wait()
@@ -248,10 +256,10 @@
 VMEM = pl.BlockSpec(memory_space=pltpu.VMEM)
 
 
-def gather_call(n_sp, n_fs, n_tp, width, tokens, w_ins, offsets, w_outs):
+def gather_call(n_sp, n_fs, n_tp, width, tokens, w_ins, offsets, w_out, conv_gain):
     rows, features = tokens.shape
     depth = w_ins[0].shape[0]
-    o_rows, o_cols = w_outs[0].shape
+    o_rows, o_cols = w_out.shape
     dma = pltpu.SemaphoreType.DMA
     return pl.pallas_call(
         functools.partial(gather_kernel, n_sp, True),
@@ -260,7 +268,7 @@
             jax.ShapeDtypeStruct((n_fs * depth, 5 * width), BF16),
             jax.ShapeDtypeStruct((n_sp,) + offsets.shape, F32),
             jax.ShapeDtypeStruct((n_tp * o_rows, n_fs * o_cols), BF16),
-            jax.ShapeDtypeStruct((n_tp * o_rows, n_fs * o_cols), BF16),
+            jax.ShapeDtypeStruct((n_tp,) + conv_gain.shape, F32),
         ],
         in_specs=[ANY] * 9,
         out_specs=[ANY] * 5,
@@ -270,16 +278,45 @@
             dma((n_sp,)), dma((n_sp,)),
             dma((6,)), dma((6,)),
             dma((n_sp - 1,)), dma((n_sp - 1,)),
-            dma((8,)),
-        ] + OUT_SEMS,
+            dma((9,)),
+        ] + OUT_SEMS + [dma((2,))],
         compiler_params=pltpu.CompilerParams(collective_id=0, has_side_effects=True),
         name="gather_inputs",
-    )(tokens, *w_ins, offsets, *w_outs)
-
-
-def compute_body(width, heads, taps, blk, tok, gain, w, off, ck, attn_out, conv_out, mean_out, proj, gated):
-    length = tok.shape[0]
-    n_rows = mean_out.shape[2]
+    )(tokens, *w_ins, offsets, w_out, conv_gain)
+
+
+def compute_body(n_sp, n_tp, width, heads, taps, blk, *refs):
+    tok, gain, w, off, ck, cgain, wa_hbm, wc_own, mixed = refs[:9]
+    attn_out, conv_out, mean_out, proj, gated, wa, wc, x_all, mean_all, send, recv, loc, wa_sem = refs[9:22]
+    length, n_rows = tok.shape[0], mean_out.shape[2]
+    gather = OutGather(wc_own, wc, refs[22:])
+    z, tp, fs = lax.axis_index("sp"), lax.axis_index("tp"), lax.axis_index("fs")
+    xn, yn, _ = plane(fs)
+    me, place, n = z * n_tp + tp, tp * n_sp + z, n_sp * n_tp
+    fetch = pltpu.make_async_copy(wa_hbm, wa, wa_sem.at[0])
+    fetch.start()
+    peers = [(me + d) % n for d in range(1, n)]
+    greet([{"sp": p // n_tp, "tp": p % n_tp} for p in peers] + [{"fs": xn}, {"fs": yn}])
+    gather.start()
+
+    def pair(k, dest, slot):
+        at = pl.ds(pl.multiple_of(dest * n_rows, n_rows), n_rows)
+        if k == 2:
+            return mean_out.at[dest], mean_all.at[slot]
+        there = pl.ds(pl.multiple_of((k * n + slot) * width, width), width)
+        return (attn_out, conv_out)[k].at[at], x_all.at[:, there]
+
+    def ship(k, sp, core):
+        src, dst = pair(k, sp * n_tp + core, place)
+        mine = jnp.logical_and(z == sp, tp == core)
+
+        @pl.when(mine)
+        def _():
+            pltpu.make_async_copy(src, dst, loc.at[k]).start()
+
+        @pl.when(jnp.logical_not(mine))
+        def _():
+            remote(src, dst, send.at[k, sp * n_tp + core], recv.at[k, place], sp=sp, tp=core).start()
 
     def project(i, _):
         at = pl.ds(pl.multiple_of(i * 128, 128), 128)
@@ -319,20 +356,21 @@
     after = jnp.where(row >= col, 1.0, 0.0).astype(BF16)
     lane = lax.broadcasted_iota(jnp.int32, (blk, width), 1)
 
-    def attend(i, _):
-        q_at = pl.ds(pl.multiple_of(i * blk, blk), blk)
-        merged = jnp.zeros((blk, width), F32)
-        for h in range(heads):
-            mine = jnp.logical_and(lane >= h * HD, lane < (h + 1) * HD)
-            q = jnp.where(mine, proj[q_at, :width].astype(F32) * HD ** (-0.5), 0.0).astype(BF16)
-
-            def piece(j, carry, total, diagonal):
-                k_at = pl.ds(pl.multiple_of(j * blk, blk), blk)
-                k = proj[k_at, width : 2 * width]
-                v = proj[k_at, 2 * width : 3 * width]
-                s = lax.dot_general(q, k, (((1,), (1,)), ((), ())), preferred_element_type=F32)
+    def attend(i):
+        q_at = pl.ds(i * blk, blk)
+        mine = [jnp.logical_and(lane >= h * HD, lane < (h + 1) * HD) for h in range(heads)]
+        q_all = proj[q_at, :width].astype(F32) * HD ** (-0.5)
+        qs = [jnp.where(m, q_all, 0.0).astype(BF16) for m in mine]
+
+        def pieces(j, state, diagonal):
+            k_at = pl.ds(pl.multiple_of(j * blk, blk), blk)
+            k = proj[k_at, width : 2 * width]
+            v = proj[k_at, 2 * width : 3 * width]
+            result = []
+            for h, (carry, total) in enumerate(state):
+                s = lax.dot_general(qs[h], k, (((1,), (1,)), ((), ())), preferred_element_type=F32)
                 s = s + off[j, h : h + 1, :]
-                keep = -(jnp.maximum(s, 0.0) + jnp.log(1.0 + jnp.exp(-jnp.abs(s))))
+                keep = jnp.minimum(-s, 0.0) - jnp.log(1.0 + jnp.exp(-jnp.abs(s)))
                 if diagonal:
                     keep = jnp.where(allowed, keep, 0.0)
                 high = keep.astype(BF16)
@@ -343,93 +381,110 @@
                 if diagonal:
                     weights = jnp.where(allowed, weights, 0.0)
                 total = total + jnp.dot(weights.astype(BF16), v, preferred_element_type=F32)
-                return carry + suffix[:, :1], total
-
-            carry, total = piece(i, jnp.zeros((blk, 1), F32), jnp.zeros((blk, width), F32), True)
-            carry, total = lax.fori_loop(
-                0, i, lambda t, c: piece(i - 1 - t, c[0], c[1], False), (carry, total)
-            )
-            merged = jnp.where(mine, total, merged)
+                result.append((carry + suffix[:, :1], total))
+            return tuple(result)
+
+        state = tuple((jnp.zeros((blk, 1), F32), jnp.zeros((blk, width), F32)) for _ in range(heads))
+        state = pieces(i, state, True)
+        if i:
+            state = lax.fori_loop(0, i, lambda t, c: pieces(i - 1 - t, c, False), state)
+        merged = state[0][1]
+        for h in range(1, heads):
+            merged = jnp.where(mine[h], state[h][1], merged)
         attn_out[q_at, :] = merged.astype(BF16)
+
+    for step, i in enumerate(reversed(range(n_sp))):
+        attend(i)
+        if step == 0:
+            for sp in range(n_sp):
+                for core in range(n_tp):
+                    ship(1, sp, core)
+                    ship(2, sp, core)
+        else:
+            for core in range(n_tp):
+                ship(0, i + 1, core)
+        if step == (n_sp - 1) // 2:
+            gather.middle()
+    gather.finish()
+    for core in range(n_tp):
+        ship(0, 0, core)
+    fetch.wait()
+
+    def arrive(k):
+        src, dst = pair(k, me, place)
+        pltpu.make_async_copy(src, dst, loc.at[k]).wait()
+        for d in range(1, n):
+            source = (me - d + n) % n
+            slot = (source % n_tp) * n_sp + source // n_tp
+            src, dst = pair(k, me, slot)
+            remote(src, dst, send.at[k, me], recv.at[k, slot], tp=1 - tp).wait_recv()
+
+    arrive(2)
+    arrive(1)
+    square = (lax.broadcasted_iota(jnp.int32, (n_rows, n_rows), 0)
+              == lax.broadcasted_iota(jnp.int32, (n_rows, n_rows), 1)).astype(F32)
+    local = [
+        lax.dot_general(square, mean_all[g], (((1,), (1,)), ((), ())),
+                        precision=lax.Precision.HIGHEST, preferred_element_type=F32)[:, :1]
+        for g in range(n)
+    ]
+    mean = sum(local) / n
+    base = n * width
+    centred = [
+        x_all[:, base + g * width : base + (g + 1) * width].astype(F32) + (local[g] - mean) for g in range(n)
+    ]
+    shift = sum(jnp.sum(c, axis=1, keepdims=True) for c in centred) / base
+    centred = [c - shift for c in centred]
+    spread = sum(jnp.sum(c * c, axis=1, keepdims=True) for c in centred) / base
+    scale = lax.rsqrt(spread + 1e-06)
+    hidden = []
+    for g, c in enumerate(centred):
+        y = c * scale * cgain[:, g * width : (g + 1) * width]
+        hidden.append((y * jax.nn.sigmoid(y)).astype(BF16))
+    hidden = jnp.concatenate(hidden, axis=1)
+    arrive(0)
+    chunk = wc_own.shape[1]
+
+    def output(c, _):
+        at = pl.ds(pl.multiple_of(c * chunk, chunk), chunk)
+        total = jnp.dot(x_all[:, :base], wa[:, at], preferred_element_type=F32)
+        total = total + jnp.dot(hidden, wc[:, at], preferred_element_type=F32)
+        mixed[:, at] = total.astype(BF16)
         return 0
 
-    lax.fori_loop(0, length // blk, attend, 0)
-
-
-def compute_call(width, heads, blk, n_dest, tok, gain, w, off, ck):
+    lax.fori_loop(0, wc.shape[1] // chunk, output, 0)
+    for d in range(1, n):
+        p = (me + d) % n
+        for k in range(3):
+            src, dst = pair(k, p, place)
+            remote(src, dst, send.at[k, p], recv.at[k, place], tp=1 - tp).wait_send()
+
+
+def compute_call(n_sp, n_tp, width, heads, blk, tok, gain, w, off, ck, cgain, wa, w_out):
     length = tok.shape[0]
-    return pl.pallas_call(
-        functools.partial(compute_body, width, heads, ck.shape[0], blk),
-        out_shape=[
-            jax.ShapeDtypeStruct((length, width), BF16),
-            jax.ShapeDtypeStruct((length, width), BF16),
-            jax.ShapeDtypeStruct((n_dest, 8, length // n_dest), F32),
-        ],
-        in_specs=[VMEM] * 5,
-        out_specs=[VMEM] * 3,
-        scratch_shapes=[pltpu.VMEM((length, 3 * width), BF16), pltpu.VMEM((length + 32, width), F32)],
-        name="branches",
-    )(tok, gain, w, off, ck)
-
-
-def exchange_kernel(n_sp, n_tp, attn, conv, mean, x_out, mean_all, send, recv, loc):
-    z, tp = lax.axis_index("sp"), lax.axis_index("tp")
-    me = z * n_tp + tp
     n = n_sp * n_tp
-    rows, cols = x_out.shape
-    width = attn.shape[1]
-    place = tp * n_sp + z
-
-    def slots(index):
-        return (
-            x_out.at[:, pl.ds(pl.multiple_of(index * width, width), width)],
-            x_out.at[:, pl.ds(pl.multiple_of(cols // 2 + index * width, width), width)],
-            mean_all.at[index],
-        )
-
-    def pieces(dest):
-        at = pl.ds(pl.multiple_of(dest * rows, rows), rows)
-        return (attn.at[at], conv.at[at], mean.at[dest])
-
-    keeps = [
-        pltpu.make_async_copy(s, d, loc.at[k]) for k, (s, d) in enumerate(zip(pieces(me), slots(place)))
-    ]
-    for copy in keeps:
-        copy.start()
-    peers = [(me + d) % n for d in range(1, n)]
-    greet([{"sp": p // n_tp, "tp": p % n_tp} for p in peers])
-    copies = []
-    for d, p in enumerate(peers):
-        for k, (s, t) in enumerate(zip(pieces(p), slots(place))):
-            copies.append(remote(s, t, send.at[d, k], recv.at[d, k], sp=p // n_tp, tp=p % n_tp))
-    for copy in copies:
-        copy.start()
-    for d in range(1, n):
-        src = (me - d + n) % n
-        for k, (s, t) in enumerate(zip(pieces(me), slots((src % n_tp) * n_sp + src // n_tp))):
-            remote(s, t, send.at[d - 1, k], recv.at[d - 1, k], sp=z, tp=1 - tp).wait_recv()
-    for copy in copies:
-        copy.wait_send()
-    for copy in keeps:
-        copy.wait()
-
-
-def exchange_call(n_sp, n_tp, attn, conv, mean):
-    n = n_sp * n_tp
-    length, width = attn.shape
+    rows = length // n
     dma = pltpu.SemaphoreType.DMA
     return pl.pallas_call(
-        functools.partial(exchange_kernel, n_sp, n_tp),
-        out_shape=[
-            jax.ShapeDtypeStruct((length // n, 2 * width * n), BF16),
-            jax.ShapeDtypeStruct((n, 8, length // n), F32),
-        ],
-        in_specs=[VMEM] * 3,
-        out_specs=[VMEM] * 2,
-        scratch_shapes=[dma((n - 1, 3)), dma((n - 1, 3)), dma((3,))],
+        functools.partial(compute_body, n_sp, n_tp, width, heads, ck.shape[0], blk),
+        out_shape=jax.ShapeDtypeStruct((rows, wa.shape[1]), BF16),
+        in_specs=[VMEM] * 6 + [ANY] * 2,
+        out_specs=VMEM,
+        scratch_shapes=[
+            pltpu.VMEM((length, width), BF16),
+            pltpu.VMEM((length, width), BF16),
+            pltpu.VMEM((n, 8, rows), F32),
+            pltpu.VMEM((length, 3 * width), BF16),
+            pltpu.VMEM((length + 32, width), F32),
+            pltpu.VMEM(wa.shape, BF16),
+            pltpu.VMEM(wa.shape, BF16),
+            pltpu.VMEM((rows, 2 * n * width), BF16),
+            pltpu.VMEM((n, 8, rows), F32),
+            dma((3, n)), dma((3, n)), dma((3,)), dma((1,)),
+        ] + OUT_SEMS,
         compiler_params=pltpu.CompilerParams(collective_id=1, has_side_effects=True),
-        name="to_positions",
-    )(attn, conv, mean)
+        name="branches",
+    )(tok, gain, w, off, ck, cgain, wa, w_out)
 
 
 def spread_shards(
@@ -447,34 +502,22 @@
     w_conv_out,
 ):
     n_sp, n_fs, n_tp = (lax.axis_size(a) for a in ("sp", "fs", "tp"))
-    z, tp = lax.axis_index("sp"), lax.axis_index("tp")
+    z = lax.axis_index("sp")
     width = w_query.shape[1] // n_sp
     heads = width // HD
     offsets = jnp.transpose(key_offset.astype(F32))
-    tok_all, w_all, off_all, wa, wc = gather_call(
+    tok_all, w_all, off_all, wa, cgain = gather_call(
         n_sp, n_fs, n_tp, width, tokens[0],
-        (w_query, w_key, w_value, w_conv_value, w_conv_gate), offsets, (w_attn_out, w_conv_out),
-    )
-    features = tokens.shape[2]
-    tok_all = tok_all.reshape(-1, features)
+        (w_query, w_key, w_value, w_conv_value, w_conv_gate), offsets, w_attn_out, conv_gain[None],
+    )
+    tok_all = tok_all.reshape(-1, tokens.shape[2])
     off = lax.dynamic_slice_in_dim(off_all, z * heads, heads, axis=1)
     taps = lax.dynamic_slice_in_dim(conv_kernel, z * width, width, axis=1)
-    attn, conv, mean = compute_call(
-        width, heads, key_offset.shape[0], n_sp * n_tp, tok_all, norm_gain[None], w_all, off, taps
-    )
-    x, means = exchange_call(n_sp, n_tp, attn, conv, mean)
-    half = x.shape[1] // 2
-    groups = n_sp * n_tp
-    local = jnp.transpose(means[:, 0, :])
-    local = local - jnp.mean(local, axis=1, keepdims=True)
-    gain = lax.all_gather(conv_gain, "tp", axis=0, tiled=True)
-    centred = (x[:, half:].astype(F32).reshape(-1, groups, width) + local[:, :, None]).reshape(-1, half)
-    centred = centred - jnp.mean(centred, axis=1, keepdims=True)
-    spread = jnp.mean(centred * centred, axis=1, keepdims=True)
-    hidden = jax.nn.silu(centred * lax.rsqrt(spread + 1e-06) * gain).astype(BF16)
-    mixed = jnp.dot(x[:, :half], wa, preferred_element_type=F32)
-    mixed = mixed + jnp.dot(hidden, wc, preferred_element_type=F32)
-    return mixed.astype(BF16)[None]
+    mixed = compute_call(
+        n_sp, n_tp, width, heads, key_offset.shape[0], tok_all, norm_gain[None], w_all, off, taps,
+        cgain.reshape(1, -1), wa, w_conv_out,
+    )
+    return mixed[None]
 
 
 def shifted(block, axis, distance):

time: 121 us -> 96.7 us (0.80)
  Pallas kernels: 106 us -> 91.2 us
  matrix products: 4.73 us -> 0 us
  other arithmetic: 4.63 us -> 1.31 us
  blocking collectives: 2.8 us -> 0 us
  local copies, waits for them, and re-layouts: 2.28 us -> 3.86 us
    pallas_call x1, Pallas kernels: 65.2 us -> 50.5 us  [gather_call(): pl.pallas_call(functools.partial(gather_kernel, n_sp, True), out_shape=[j...]
    dot_general x2 -> x0, matrix products: 4.73 us -> none  [the longest x1 3 us: spread_shards(): mixed = jnp.dot(x[:, :half], wa, preferred_element_type=F32)]
    reduce_sum x3 -> x0, other arithmetic: 3.28 us -> none  [the longest x1 1.27 us: spread_shards(): centred = centred - jnp.mean(centred, axis=1, keepdims=True)]
    all_gather x1 -> x0, blocking collectives: 2.8 us -> none  [spread_shards(): gain = lax.all_gather(conv_gain, 'tp', axis=0, tiled=True)]
    unnamed x8 -> x3, local copies, waits for them, and re-layouts: 0.02 us -> 1.89 us
    pallas_call x2 -> x1, Pallas kernels: 40.3 us -> 40.7 us  [compute_call(): pl.pallas_call(functools.partial(compute_body, n_sp, n_tp, width, heads,...]
where the time goes in v2:
time: 96.7 us; the launch traced here: 96.4 us
  Pallas kernels  91.2 us (94%)
  local copies, waits for them, and re-layouts  3.86 us (4%)
  other arithmetic  1.31 us (1%)
    pallas_call x1, Pallas kernels, gather_call(): pl.pallas_call(functools.partial(gather_kernel, n_sp, True), out_shape=[j...  50.5 us
    pallas_call x1, Pallas kernels, compute_call(): pl.pallas_call(functools.partial(compute_body, n_sp, n_tp, width, heads,...  40.7 us

profile of v2, /device:TPU:0, one launch (start us, length us, event | category | flops | bytes accessed | tf_op | source)
XLA Modules:
  0.0 96.4 jit_solution(3846669030414537220)
XLA Ops:
  0.0 0.0 copy-start
  0.0 1.3 %convert_bitcast_fusion.refs_6_ = f32[8,256]{1,0:T(8,128)} fusion(bf16[256,8]{0,1:T(8,128)(2,1)} %param.19), kind=kLoop, calls=%fused_computation | loop fusion | flops 2048 | bytes 12288 | tf_op jit(solution)/shard_map/transpose | solution.py:508
  1.3 0.0 copy-done
  1.3 0.6 constant_dynamic-slice_fusion.refs_4_
  1.9 50.5 %gather_inputs.1 = (bf16[4,2,128,2048]{3,2,1,0:T(8,128)(2,1)}, bf16[2048,640]{1,0:T(8,128)(2,1)}, f32[4,8,256]{2,1,0:T(8,128)}, bf16[1024,2048]{1,0:T(8,128)(2,1)}, f32[2,1,512]{2,1,0:T(1,128)}) custom-call(bf16[128,2048]{1,0:T(8,128)(2,1)} %bitcast.10, bf16[512,512]{1,0:T(8,128)(2,1)} %refs_1_.1, bf16[512,512]{1,0:T(8,128)(2,1)} %refs_2_.1, ...), custom_call_target="tpu_custom_call" | custom-call | tf_op jit(solution)/shard_map/gather_inputs/pallas_call | solution.py:264
  52.4 1.4 %constant_dynamic-slice_fusion.1.refs_3_ = f32[4,2,256]{2,1,0:T(2,128)} fusion(f32[4,8,256]{2,1,0:T(8,128)} %get-tuple-element.12, s32[]{:T(128)S(6)} %select_n.6), kind=kLoop, calls=%fused_computation.2 | loop fusion | bytes 16388 | tf_op jit(solution)/shard_map/dynamic_slice | solution.py:514
  53.8 40.7 %branches.1 = bf16[128,2048]{1,0:T(8,128)(2,1)} custom-call(bf16[1024,2048]{1,0:T(8,128)(2,1)} %bitcast.8, f32[1,2048]{1,0:T(1,128)} %bitcast.11, bf16[2048,640]{1,0:T(8,128)(2,1)} %get-tuple-element.11.refs_2_, f32[4,2,256]{2,1,0:T(2,128)} %constant_dynamic-slice_fusion.1.refs_3_, f32[31,128]{1,0:T(8,128)} %constant_dynamic-slice_fusion.refs_4_, ...), custom_call_target="tpu_custom_call" | custom-call | tf_op jit(solution)/shard_map/branches/pallas_call | solution.py:468
  94.5 1.9 %copy.14 = bf16[1,128,2048]{2,1,0:T(8,128)(2,1)} copy(bf16[1,128,2048]{2,1,0:T(8,128)(2,1)} %bitcast.9) | data formatting | bytes 1048576
Async XLA Ops:
  0.0 1.3 %copy-start = (f32[31,512]{1,0:T(8,128)S(1)}, f32[31,512]{1,0:T(8,128)}, u32[]{:S(2)}) copy-start(f32[31,512]{1,0:T(8,128)} %param.20) | copy-start | bytes 190468

commit v3 on v2

--- a/solution.py
+++ b/solution.py
@@ -205,6 +205,9 @@
         gather.start()
 
     for dist in range(1, n_sp):
+        if with_out and dist == n_sp - 1:
+            gather.middle()
+
         @pl.when(z >= dist)
         def _():
             block = (z - dist + n_sp) % n_sp
@@ -228,7 +231,6 @@
     for s, owner, h in arrivals[2:]:
         send_w(part(owner, h), owner, h, s, xn).wait_recv()
     if with_out:
-        gather.middle()
         gather.finish()
     for copy in first + relay:
         copy.wait_send()
@@ -286,14 +288,23 @@
 
 
 def compute_body(n_sp, n_tp, width, heads, taps, blk, *refs):
-    tok, gain, w, off, ck, cgain, wa_hbm, wc_own, mixed = refs[:9]
-    attn_out, conv_out, mean_out, proj, gated, wa, wc, x_all, mean_all, send, recv, loc, wa_sem = refs[9:22]
+    tok_hbm, gain, w_hbm, off, ck, cgain, wa_hbm, wc_own, mixed = refs[:9]
+    attn_out, conv_out, mean_out, proj, gated, wa, wc, x_all, mean_all, send, recv, loc, wa_sem, tok, w, tok_sem = refs[9:25]
     length, n_rows = tok.shape[0], mean_out.shape[2]
-    gather = OutGather(wc_own, wc, refs[22:])
+    gather = OutGather(wc_own, wc, refs[25:])
     z, tp, fs = lax.axis_index("sp"), lax.axis_index("tp"), lax.axis_index("fs")
     xn, yn, _ = plane(fs)
     me, place, n = z * n_tp + tp, tp * n_sp + z, n_sp * n_tp
     fetch = pltpu.make_async_copy(wa_hbm, wa, wa_sem.at[0])
+    load_w = pltpu.make_async_copy(w_hbm, w, wa_sem.at[1])
+
+    def load(i):
+        at = pl.ds(pl.multiple_of(i * 128, 128), 128)
+        return pltpu.make_async_copy(tok_hbm.at[at], tok.at[at], tok_sem.at[i])
+
+    load_w.start()
+    for i in range(length // 128):
+        load(i).start()
     fetch.start()
     peers = [(me + d) % n for d in range(1, n)]
     greet([{"sp": p // n_tp, "tp": p % n_tp} for p in peers] + [{"fs": xn}, {"fs": yn}])
@@ -320,6 +331,7 @@
 
     def project(i, _):
         at = pl.ds(pl.multiple_of(i * 128, 128), 128)
+        load(i).wait()
         x = tok[at, :].astype(F32)
         normed = (x * lax.rsqrt(jnp.mean(x * x, axis=1, keepdims=True) + 1e-06) * gain[...]).astype(BF16)
         out = jnp.dot(normed, w[...], preferred_element_type=F32).astype(BF16)
@@ -330,6 +342,7 @@
         return 0
 
     gated[pl.ds(0, 32), :] = jnp.zeros((32, width), F32)
+    load_w.wait()
     lax.fori_loop(0, length // 128, project, 0)
 
     ones = jnp.full((8, width), 1.0 / width, F32)
@@ -340,7 +353,7 @@
         total = jnp.zeros((n_rows, width), F32)
         for tap in range(taps):
             lo = 32 - (taps - 1) + tap
-            total = total + ck[tap : tap + 1, :] * window[lo : lo + n_rows]
+            total = total + ck[tap : tap + 1, pl.ds(pl.multiple_of(z * width, width), width)] * window[lo : lo + n_rows]
         local = jnp.mean(total, axis=1, keepdims=True)
         conv_out[pl.ds(base, n_rows), :] = (total - local).astype(BF16)
         mean_out[i] = lax.dot_general(
@@ -369,7 +382,7 @@
             result = []
             for h, (carry, total) in enumerate(state):
                 s = lax.dot_general(qs[h], k, (((1,), (1,)), ((), ())), preferred_element_type=F32)
-                s = s + off[j, h : h + 1, :]
+                s = s + off[j, pl.ds(z * heads + h, 1), :]
                 keep = jnp.minimum(-s, 0.0) - jnp.log(1.0 + jnp.exp(-jnp.abs(s)))
                 if diagonal:
                     keep = jnp.where(allowed, keep, 0.0)
@@ -468,7 +481,7 @@
     return pl.pallas_call(
         functools.partial(compute_body, n_sp, n_tp, width, heads, ck.shape[0], blk),
         out_shape=jax.ShapeDtypeStruct((rows, wa.shape[1]), BF16),
-        in_specs=[VMEM] * 6 + [ANY] * 2,
+        in_specs=[ANY, VMEM, ANY] + [VMEM] * 3 + [ANY] * 2,
         out_specs=VMEM,
         scratch_shapes=[
             pltpu.VMEM((length, width), BF16),
@@ -480,7 +493,10 @@
             pltpu.VMEM(wa.shape, BF16),
             pltpu.VMEM((rows, 2 * n * width), BF16),
             pltpu.VMEM((n, 8, rows), F32),
-            dma((3, n)), dma((3, n)), dma((3,)), dma((1,)),
+            dma((3, n)), dma((3, n)), dma((3,)), dma((2,)),
+            pltpu.VMEM(tok.shape, BF16),
+            pltpu.VMEM(w.shape, BF16),
+            dma((length // 128,)),
         ] + OUT_SEMS,
         compiler_params=pltpu.CompilerParams(collective_id=1, has_side_effects=True),
         name="branches",
@@ -502,7 +518,6 @@
     w_conv_out,
 ):
     n_sp, n_fs, n_tp = (lax.axis_size(a) for a in ("sp", "fs", "tp"))
-    z = lax.axis_index("sp")
     width = w_query.shape[1] // n_sp
     heads = width // HD
     offsets = jnp.transpose(key_offset.astype(F32))
@@ -511,10 +526,8 @@
         (w_query, w_key, w_value, w_conv_value, w_conv_gate), offsets, w_attn_out, conv_gain[None],
     )
     tok_all = tok_all.reshape(-1, tokens.shape[2])
-    off = lax.dynamic_slice_in_dim(off_all, z * heads, heads, axis=1)
-    taps = lax.dynamic_slice_in_dim(conv_kernel, z * width, width, axis=1)
     mixed = compute_call(
-        n_sp, n_tp, width, heads, key_offset.shape[0], tok_all, norm_gain[None], w_all, off, taps,
+        n_sp, n_tp, width, heads, key_offset.shape[0], tok_all, norm_gain[None], w_all, off_all, conv_kernel,
         cgain.reshape(1, -1), wa, w_conv_out,
     )
     return mixed[None]

time: 96.7 us -> 90.3 us (0.934)
  Pallas kernels: 91.2 us -> 86.9 us
  local copies, waits for them, and re-layouts: 3.86 us -> 1.88 us
    pallas_call x1, Pallas kernels: 50.5 us -> 47.7 us  [gather_call(): pl.pallas_call(functools.partial(gather_kernel, n_sp, True), out_shape=[j...]
    dynamic_slice x2 -> x0, local copies, waits for them, and re-layouts: 1.98 us -> none  [the longest x1 1.37 us: spread_shards(): off = lax.dynamic_slice_in_dim(off_all, z * heads, heads, axis=1)]
    pallas_call x1, Pallas kernels: 40.7 us -> 39.2 us  [compute_call(): pl.pallas_call(functools.partial(compute_body, n_sp, n_tp, width, heads,...]
where the time goes in v3:
time: 90.3 us; the launch traced here: 90.1 us
  Pallas kernels  86.9 us (96%)
  local copies, waits for them, and re-layouts  1.88 us (2%)
  other arithmetic  1.29 us (1%)
    pallas_call x1, Pallas kernels, gather_call(): pl.pallas_call(functools.partial(gather_kernel, n_sp, True), out_shape=[j...  47.7 us
    pallas_call x1, Pallas kernels, compute_call(): pl.pallas_call(functools.partial(compute_body, n_sp, n_tp, width, heads,...  39.2 us
    unnamed x1, local copies, waits for them, and re-layouts  1.88 us

profile of v3, /device:TPU:0, one launch (start us, length us, event | category | flops | bytes accessed | tf_op | source)
XLA Modules:
  0.0 90.1 jit_solution(4512423742090721357)
XLA Ops:
  0.0 1.3 %convert_bitcast_fusion.refs_6_ = f32[8,256]{1,0:T(8,128)} fusion(bf16[256,8]{0,1:T(8,128)(2,1)} %param.19), kind=kLoop, calls=%fused_computation | loop fusion | flops 2048 | bytes 12288 | tf_op jit(solution)/shard_map/transpose | solution.py:523
  1.3 47.7 %gather_inputs.1 = (bf16[4,2,128,2048]{3,2,1,0:T(8,128)(2,1)}, bf16[2048,640]{1,0:T(8,128)(2,1)}, f32[4,8,256]{2,1,0:T(8,128)}, bf16[1024,2048]{1,0:T(8,128)(2,1)}, f32[2,1,512]{2,1,0:T(1,128)}) custom-call(bf16[128,2048]{1,0:T(8,128)(2,1)} %bitcast.10, bf16[512,512]{1,0:T(8,128)(2,1)} %refs_1_.1, bf16[512,512]{1,0:T(8,128)(2,1)} %refs_2_.1, ...), custom_call_target="tpu_custom_call" | custom-call | tf_op jit(solution)/shard_map/gather_inputs/pallas_call | solution.py:266
  49.0 39.2 %branches.1 = bf16[128,2048]{1,0:T(8,128)(2,1)} custom-call(bf16[1024,2048]{1,0:T(8,128)(2,1)} %bitcast.8, f32[1,2048]{1,0:T(1,128)} %bitcast.11, bf16[2048,640]{1,0:T(8,128)(2,1)} %get-tuple-element.11.refs_2_, f32[4,8,256]{2,1,0:T(8,128)} %get-tuple-element.12.refs_3_, f32[31,512]{1,0:T(8,128)} %refs_4_.3, f32[1,1024]{1,0:T(1,128)} %bitcast.12, ...), custom_call_target="tpu_custom_call" | custom-call | tf_op jit(solution)/shard_map/branches/pallas_call | solution.py:481
  88.2 1.9 %copy.14 = bf16[1,128,2048]{2,1,0:T(8,128)(2,1)} copy(bf16[1,128,2048]{2,1,0:T(8,128)(2,1)} %bitcast.9) | data formatting | bytes 1048576
